TPU v7x, 32 devices: a whole 2x2x4 slice. The times are simulated.
32 devices in a mesh: sp: 8 (over z, x), tp: 4 (over y, core).
Axes of the slice: x: 2, y: 2, z: 4, core: 2. Of those that a mesh axis runs over, the one named last changes fastest.
Arguments:
- probe_vectors: bfloat16 [1024, 2048], P('sp', 'tp'), may hold values from -6 to 6
- address_vectors: bfloat16 [1024, 2048], P('sp', 'tp'), may hold values from -6 to 6
- content_vectors: bfloat16 [1024, 2048], P('sp', 'tp'), may hold values from -6 to 6
- storage_raw_signal: float32 [16, 1024], P('tp', 'sp'), may hold values from -8 to 4
- fade_raw_signal: float32 [16, 1024], P('tp', 'sp'), may hold values from -6 to 6
- channel_fade_exponent: float32 [16], P('tp'), may hold values from -9 to 0
- extra_fade_amount: float32 [16, 1024], P('tp', 'sp'), may hold values from -1 to 0
- sequence_label: int32 [1024], P('sp'), may hold values from 0 to 2, never falling along the last dimension, each value on 1 to 768 neighbouring positions
- exit_valve_raw_signal: bfloat16 [1024, 2048], P('sp', 'tp'), may hold values from -6 to 6
- final_projection_matrix: bfloat16 [2048, 2048], P('tp'), may hold values from -0.125 to 0.125
- incoming_rows_matrix: bfloat16 [1024, 2048], P('sp', 'tp'), may hold values from -48 to 48
- initial_rescale_factor: float32 [2048], P('tp'), may hold values from 0 to 3
- specialist_picks: int32 [1024, 2], P('sp'), may hold values from 0 to 7, all different within a row; in each aligned block of 128 rows (0 to 127, 128 to 255, ...) at most 36 rows name the same one
- picked_specialist_share: bfloat16 [1024, 2], P('sp'), may hold values from 0.29882812 to 1.1953125
- specialist_valve_matrix: bfloat16 [8, 2048, 4096], P('sp', None, 'tp'), may hold values from -0.125 to 0.125
- specialist_raising_matrix: bfloat16 [8, 2048, 4096], P('sp', None, 'tp'), may hold values from -0.125 to 0.125
- specialist_lowering_matrix: bfloat16 [8, 4096, 2048], P('sp', 'tp'), may hold values from -0.09375 to 0.09375
- common_valve_matrix: bfloat16 [2048, 512], P(None, 'tp'), may hold values from -0.125 to 0.125
- common_raising_matrix: bfloat16 [2048, 512], P(None, 'tp'), may hold values from -0.125 to 0.125
- common_lowering_matrix: bfloat16 [512, 2048], P('tp'), may hold values from -0.25 to 0.25
- latter_rescale_factor: float32 [2048], P('tp'), may hold values from 0.1 to 1.9
Outputs:
- result: bfloat16 [1024, 2048], P('sp', 'tp')
Inputs may be any that keep to these rules, and one draw needn't show every extreme that they name: `sequence_label`: document numbers never fall; a document has 1 to 768 positions, one exactly 768. `specialist_picks`: each row names 2 different experts; among the rows of one index of sp no expert is named more than 36 times, a bound that some block reaches.
All inputs are finite; a program needn't handle non-finite values.
Results may differ from a plain program's by a relative error of at most 0.018.
Values may be sent and summed in bfloat16 or wider, within the bound.
A program may use at most 64 MiB of HBM per device.

v0:
```python
import jax
import jax.numpy as jnp
from jax import lax
from jax.sharding import PartitionSpec as P

DK = 128
DV = 128
BLOCK = 64


HIGH = lax.Precision.HIGHEST
ALPHA = 2.0**0.25


def entering(value, axis, join, neutral):
    place = lax.axis_index(axis)
    gathered = jax.tree.map(
        lambda a, kind: lax.all_gather(a.astype(kind), axis),
        value,
        (jnp.bfloat16, jnp.bfloat16, jnp.bfloat16, jnp.bfloat16),
    )
    state = jax.tree.map(lambda a, e: jnp.zeros_like(a) + jnp.asarray(e, a.dtype), value, neutral)

    def one(hop, state):
        return join(
            state,
            jax.tree.map(
                lambda a, own: lax.dynamic_index_in_dim(a, hop, 0, False).astype(own.dtype),
                gathered,
                value,
            ),
        )

    return lax.fori_loop(0, place, one, state)


def unit_rows(array):
    return array * lax.rsqrt(jnp.sum(array * array, -1, keepdims=True) + 1e-06)


def matmul_high(form, left, right):
    return jnp.einsum(form, left, right, precision=HIGH)


def feature_norm(summed, gain):
    width = summed.shape[-1] * lax.axis_size("tp")
    totals, squares = lax.psum((jnp.sum(summed, -1), jnp.sum(summed * summed, -1)), "tp")
    row_mean = totals / width
    row_var = squares / width - row_mean * row_mean
    return (summed - row_mean[:, None]) * lax.rsqrt(row_var[:, None] + 1e-05) * gain


def compose(earlier, later):
    first_map, first_shift, first_doc, first_last = earlier
    second_map, second_shift, second_doc, second_last = later
    joined = ((second_doc == first_last) | (first_last < 0) | (second_doc < 0)).astype(jnp.float32)
    new_map = joined * matmul_high("hij,hjk->hik", second_map, first_map)
    new_shift = joined * matmul_high("hij,hjk->hik", second_map, first_shift) + second_shift
    new_doc = jnp.where(first_doc < 0, second_doc, first_doc)
    new_last = jnp.where(second_last < 0, first_last, second_last)
    return (new_map, new_shift, new_doc, new_last)


def block_pass(query_unit, key_unit, write_gate, decay_logarithm, segment, values_in, initial):
    heads_here, blocks, block_len, key_depth = query_unit.shape
    cumulative = jnp.cumsum(decay_logarithm, -1)
    before = jnp.concatenate([segment[:1, 0], segment[:-1, -1]])
    carried = (segment == before[:, None]).astype(jnp.float32)
    same_doc = segment[:, :, None] == segment[:, None, :]
    offsets = jnp.arange(block_len)
    lower_tri = offsets[:, None] >= offsets[None, :]
    strict = offsets[:, None] > offsets[None, :]
    log_gap = cumulative[..., :, None] - cumulative[..., None, :]
    reach_mask = jnp.where(lower_tri & same_doc, jnp.exp(jnp.where(lower_tri, log_gap, 0.0)), 0.0)
    weighted_keys = key_unit * write_gate[..., None]
    coupling = jnp.where(
        strict, matmul_high("hncd,hnsd->hncs", weighted_keys, key_unit) * reach_mask, 0.0
    )
    identity_block = jnp.eye(block_len, dtype=jnp.float32)
    inverse = identity_block - coupling
    nil_power = coupling
    for squaring in range(block_len.bit_length() - 2):
        nil_power = matmul_high("hncs,hnst->hnct", nil_power, nil_power)
        inverse = matmul_high("hncs,hnst->hnct", inverse, identity_block + nil_power)
    growth = jnp.exp(cumulative) * carried
    update = matmul_high("hncs,hnse->hnce", inverse, values_in * write_gate[..., None])
    correction = matmul_high("hncs,hnsd->hncd", inverse, weighted_keys * growth[..., None])
    final_growth = jnp.exp(cumulative[..., -1]) * (segment[:, -1] == before).astype(jnp.float32)
    tail_decay = jnp.exp(cumulative[..., -1:] - cumulative) * (segment == segment[:, -1:]).astype(
        jnp.float32
    )
    tail_keys = key_unit * tail_decay[..., None]
    query_grown = query_unit * growth[..., None]
    local_scores = matmul_high("hncd,hnsd->hncs", query_unit, key_unit) * reach_mask

    def advance(carry_state, inputs):
        grown_query, block_corr, block_update, block_keys, block_scores, block_fade = inputs
        fresh_values = block_update - matmul_high("hcd,hde->hce", block_corr, carry_state)
        next_state = carry_state * block_fade[:, None, None] + matmul_high(
            "hcd,hce->hde", block_keys, fresh_values
        )
        block_out = matmul_high("hcd,hde->hce", grown_query, carry_state) + matmul_high(
            "hcs,hse->hce", block_scores, fresh_values
        )
        return (next_state, block_out)

    inputs = tuple(
        (
            jnp.moveaxis(array, 1, 0)
            for array in (query_grown, correction, update, tail_keys, local_scores, final_growth)
        )
    )
    final_state, outputs = lax.scan(advance, initial, inputs)
    outputs = jnp.moveaxis(outputs, 0, 1).reshape(heads_here, blocks * block_len, -1)
    return (final_state, outputs)


def shards(
    probe_vectors,
    address_vectors,
    content_vectors,
    storage_raw_signal,
    fade_raw_signal,
    channel_fade_exponent,
    extra_fade_amount,
    sequence_label,
    exit_valve_raw_signal,
    final_projection_matrix,
    incoming_rows_matrix,
    initial_rescale_factor,
    specialist_picks,
    picked_specialist_share,
    specialist_valve_matrix,
    specialist_raising_matrix,
    specialist_lowering_matrix,
    common_valve_matrix,
    common_raising_matrix,
    common_lowering_matrix,
    latter_rescale_factor,
):
    tokens_here = probe_vectors.shape[0]
    heads_here = storage_raw_signal.shape[0]
    blocks = tokens_here // BLOCK

    def split_heads(array, width):
        moved = jnp.transpose(
            array.astype(jnp.float32).reshape(tokens_here, heads_here, width), (1, 0, 2)
        )
        return moved.reshape(heads_here, blocks, BLOCK, width)

    query_unit = unit_rows(split_heads(probe_vectors, DK)) * DK ** (-0.5)
    key_unit = unit_rows(split_heads(address_vectors, DK))
    value_rows = split_heads(content_vectors, DV)
    write_gate = jax.nn.sigmoid(storage_raw_signal).reshape(heads_here, blocks, BLOCK)
    decay_logarithm = (
        extra_fade_amount
        - jnp.exp(channel_fade_exponent)[:, None] * jax.nn.softplus(fade_raw_signal)
    ).reshape(heads_here, blocks, BLOCK)
    segment = sequence_label.astype(jnp.float32).reshape(blocks, BLOCK)
    extended = jnp.concatenate(
        [value_rows, jnp.zeros((heads_here, blocks, BLOCK, DK), jnp.float32)], -1
    )
    identity_state = jnp.broadcast_to(jnp.eye(DK, dtype=jnp.float32), (heads_here, DK, DK))
    start_state = jnp.concatenate(
        [jnp.zeros((heads_here, DK, DV), jnp.float32), identity_state], -1
    )
    summary, local_out = block_pass(
        query_unit, key_unit, write_gate, decay_logarithm, segment, extended, start_state
    )
    first_doc = segment[0, 0]
    last_doc = segment[-1, -1]
    empty_doc = jnp.full((), -1.0, jnp.float32)
    prefix = entering(
        (summary[..., DV:], summary[..., :DV], first_doc, last_doc),
        "sp",
        compose,
        (identity_state, jnp.zeros((heads_here, DK, DV), jnp.float32), empty_doc, empty_doc),
    )
    incoming = prefix[1] * (first_doc == prefix[3]).astype(jnp.float32)
    memory_layer_result = local_out[..., :DV] + matmul_high(
        "hcd,hde->hce", local_out[..., DV:], incoming
    )
    scaled = memory_layer_result * lax.rsqrt(
        jnp.mean(memory_layer_result * memory_layer_result, -1, keepdims=True) + 1e-06
    )
    token_major = jnp.transpose(scaled, (1, 0, 2)).reshape(tokens_here, heads_here * DV)
    heads_out = (token_major * jax.nn.silu(exit_valve_raw_signal.astype(jnp.float32))).astype(
        jnp.bfloat16
    )
    partial_proj = jnp.dot(heads_out, final_projection_matrix, preferred_element_type=jnp.float32)
    projected = lax.psum_scatter(
        partial_proj.astype(jnp.bfloat16), "tp", scatter_dimension=1, tiled=True
    ).astype(jnp.float32)
    middle = feature_norm(
        ALPHA * incoming_rows_matrix.astype(jnp.float32) + projected, initial_rescale_factor
    ).astype(jnp.bfloat16)
    top = specialist_picks.shape[1]
    local_experts = specialist_valve_matrix.shape[0]
    experts_all = local_experts * lax.axis_size("sp")
    capacity = max(2, 9 * tokens_here * top // (8 * experts_all))
    picks = tokens_here * top
    flat_routes = specialist_picks.reshape(picks)
    one_hot = (flat_routes[:, None] == jnp.arange(experts_all, dtype=jnp.int32)[None, :]).astype(
        jnp.int32
    )
    rank_in = jnp.sum(jnp.cumsum(one_hot, 0) * one_hot, 1) - 1
    slot_of = flat_routes * capacity + rank_in
    owner = (
        jnp.full((experts_all * capacity,), picks, jnp.int32)
        .at[slot_of]
        .set(jnp.arange(picks, dtype=jnp.int32))
    )
    live = owner < picks
    safe_owner = jnp.minimum(owner, picks - 1)
    source_row = safe_owner // top
    slot_weight = jnp.where(
        live, picked_specialist_share.reshape(picks)[safe_owner], jnp.zeros((), jnp.bfloat16)
    )
    slot_shared = jnp.where(live & (safe_owner % top == 0), 1.0, 0.0).astype(jnp.bfloat16)
    slot_info = jnp.stack([slot_weight, slot_shared], -1).reshape(experts_all, capacity, 2)
    whole = lax.all_gather(middle, "tp", axis=1, tiled=True)
    sent = jnp.where(live[:, None], whole[source_row], jnp.zeros((), jnp.bfloat16)).reshape(
        experts_all, capacity, -1
    )
    arrived = lax.all_to_all(sent, "sp", split_axis=0, concat_axis=0, tiled=True)
    info = lax.all_to_all(slot_info, "sp", split_axis=0, concat_axis=0, tiled=True)
    slot_count = arrived.shape[1]
    sources = arrived.shape[0] // local_experts
    grouped = arrived.reshape(sources, local_experts, slot_count, arrived.shape[2])
    info_grouped = info.astype(jnp.float32).reshape(sources, local_experts, slot_count, 2)
    inputs_e = grouped[:, 0].reshape(sources * slot_count, -1)
    weight_e = info_grouped[:, 0, :, 0].reshape(-1, 1)
    shared_e = info_grouped[:, 0, :, 1].reshape(-1, 1)
    gate_e = jnp.dot(inputs_e, specialist_valve_matrix[0], preferred_element_type=jnp.float32)
    up_e = jnp.dot(inputs_e, specialist_raising_matrix[0], preferred_element_type=jnp.float32)
    hidden_e = (jax.nn.silu(gate_e) * up_e * weight_e).astype(jnp.bfloat16)
    shared_g = jnp.dot(inputs_e, common_valve_matrix, preferred_element_type=jnp.float32)
    shared_u = jnp.dot(inputs_e, common_raising_matrix, preferred_element_type=jnp.float32)
    shared_hidden = (jax.nn.silu(shared_g) * shared_u * shared_e).astype(jnp.bfloat16)
    partial_out = jnp.dot(
        hidden_e, specialist_lowering_matrix[0], preferred_element_type=jnp.float32
    )
    partial_out = partial_out + jnp.dot(
        shared_hidden, common_lowering_matrix, preferred_element_type=jnp.float32
    )
    results = partial_out.reshape(sources, 1, slot_count, -1)
    partials = results.reshape(sources, slot_count, -1)
    summed = lax.psum_scatter(partials.astype(jnp.bfloat16), "tp", scatter_dimension=2, tiled=True)
    returned = lax.all_to_all(summed, "sp", split_axis=0, concat_axis=0, tiled=True)
    per_route = (
        returned.reshape(experts_all * capacity, -1)[slot_of]
        .astype(jnp.float32)
        .reshape(tokens_here, top, -1)
    )
    mixture = jnp.sum(per_route, 1)
    second_sum = ALPHA * middle.astype(jnp.float32) + mixture
    return feature_norm(second_sum, latter_rescale_factor).astype(jnp.bfloat16)


def solution(mesh):
    placed = (
        P("sp", "tp"),
        P("sp", "tp"),
        P("sp", "tp"),
        P("tp", "sp"),
        P("tp", "sp"),
        P("tp"),
        P("tp", "sp"),
        P("sp"),
        P("sp", "tp"),
        P("tp", None),
        P("sp", "tp"),
        P("tp"),
        P("sp", None),
        P("sp", None),
        P("sp", None, "tp"),
        P("sp", None, "tp"),
        P("sp", "tp", None),
        P(None, "tp"),
        P(None, "tp"),
        P("tp", None),
        P("tp"),
    )
    return jax.shard_map(
        shards, mesh=mesh, in_specs=placed, out_specs=P("sp", "tp"), check_vma=False
    )
```

profile of v0, /device:TPU:0, one launch (start us, length us, event | category | flops | bytes accessed | tf_op | source)
XLA Modules:
  0.0 313.5 jit_solution(83360906726742939)
XLA Ops:
  15.4 1.3 compare_convert_fusion.2
  17.5 1.3 convolution_bitcast_fusion.2
  20.8 2.3 fusion.36
  23.1 2.1 multiply_bitcast_fusion.1
  25.2 7.6 %while.27 = (s32[]{:T(128)}, f32[4,128,256]{2,1,0:T(8,128)S(1)}, f32[2,4,64,256]{3,2,1,0:T(8,128)}, f32[2,4]{1,0:T(2,128)S(1)}, f32[2,4,64,128]{3,2,0,1:T(8,128)...) while((s32[]{:T(128)}, f32[4,128,256]{2,1,0:T(8,128)S(1)}, ...), condition=%wide.region_4.5_spmd, body=%wide.region_3.4_spmd.sunk | while | flops 352714752 | bytes 10226433 | solution.py:113
  25.2 1.4 convolution_subtract_fusion.2
  29.0 1.4 convolution_subtract_fusion.2
  37.1 1.4 dynamic-update-slice.1
  38.5 23.1 %all-reduce.6 = (bf16[8]{0:T(256)(128)(2,1)S(1)}, bf16[8]{0:T(256)(128)(2,1)S(1)}) all-reduce(bf16[8]{0:T(256)(128)(2,1)S(1)} %dynamic-update-slice, bf16[8]{0:T(256)(128)(2,1)S(1)} %dynamic-update-slice.1), channel_id=1, replica_groups=mesh['sp'=8,'tp'=4] {'sp'}, use_global_device_ids=true, to_apply=%add.2 | all-reduce | flops 16 | bytes 64
  63.5 13.5 %all-gather.6.cloned.1.call-done = bf16[32,128,128]{2,1,0:T(8,128)(2,1)} async-done(((bf16[4,128,128]{2,1,0:T(8,128)(2,1)}), bf16[32,128,128]{2,1,0:T(8,128)(2,1)}) %all-gather.6.cloned.1.call-update) | async-done | bytes 1048592 | tf_op jit(solution)/shard_map/all_gather | solution.py:18
  76.9 41.1 %all-gather.8.cloned.1.call-done = bf16[32,128,128]{2,1,0:T(8,128)(2,1)} async-done(((bf16[4,128,128]{2,1,0:T(8,128)(2,1)}), bf16[32,128,128]{2,1,0:T(8,128)(2,1)}) %all-gather.8.cloned.1.call-update) | async-done | bytes 1048592 | tf_op jit(solution)/shard_map/all_gather | solution.py:18
  119.8 1.3 convolution_convert_fusion
  121.4 1.4 scatter_custom_fusion
  122.8 2.4 gather_fusion.1
  126.0 39.2 %all-to-all-start.1 = ((bf16[8,36,2]{1,2,0:T(2,128)(2,1)}), bf16[8,36,2]{1,2,0:T(2,128)(2,1)S(1)}, u32[]{:S(2)}, u32[]{:S(2)}) async-start(bf16[8,36,2]{1,2,0:T(2,128)(2,1)} %copy.101), calls=%async_computation.2 | async-start | bytes 8192 | tf_op jit(solution)/shard_map/all_to_all | solution.py:226
  165.3 12.2 %reduce-scatter.3.cloned.1.call-done = bf16[128,512]{1,0:T(8,128)(2,1)} async-done(((bf16[128,2048]{1,0:T(8,128)(2,1)}), bf16[128,512]{1,0:T(8,128)(2,1)}) %reduce-scatter.3.cloned.1.call-update) | async-done | bytes 131088 | tf_op jit(solution)/shard_map/reduce_scatter | solution.py:191
  178.5 5.8 %all-reduce.5 = (f32[128]{0:T(128)S(1)}, f32[128]{0:T(128)S(1)}) all-reduce(f32[128]{0:T(128)S(1)} %get-tuple-element.166, f32[128]{0:T(128)S(1)} %get-tuple-element.165), channel_id=1, replica_groups=mesh['sp'=8,'tp'=4] {'tp'}, use_global_device_ids=true, to_apply=%region_12.13 | all-reduce | flops 256 | bytes 2048 | tf_op jit(solution)/shard_map/psum | solution.py:47
  185.3 6.8 %all_gather.35 = bf16[128,2048]{1,0:T(8,128)(2,1)S(1)} all-gather(bf16[128,512]{1,0:T(8,128)(2,1)S(1)} %multiply_convert_fusion.1), channel_id=1, replica_groups=mesh['sp'=8,'tp'=4] {'tp'}, dimensions={1}, use_global_device_ids=true | all-gather | bytes 655360 | tf_op jit(solution)/shard_map/all_gather | solution.py:221
  192.1 3.0 gather_fusion
  195.1 1.4 gather.12
  196.4 1.2 broadcast_select_fusion
  197.7 5.5 %all-to-all-start = ((bf16[8,36,2048]{2,1,0:T(8,128)(2,1)}), bf16[8,36,2048]{2,1,0:T(8,128)(2,1)}, u32[]{:S(2)}, u32[]{:S(2)}) async-start(bf16[8,36,2048]{2,1,0:T(8,128)(2,1)} %broadcast_select_fusion), calls=%async_computation.1 | async-start | bytes 2621440 | tf_op jit(solution)/shard_map/all_to_all | solution.py:225
  203.5 31.8 %all-to-all-done = bf16[8,36,2048]{2,1,0:T(8,128)(2,1)} async-done(((bf16[8,36,2048]{2,1,0:T(8,128)(2,1)}), bf16[8,36,2048]{2,1,0:T(8,128)(2,1)}, u32[]{:S(2)}, u32[]{:S(2)}) %all-to-all-start) | async-done | bytes 1179680 | tf_op jit(solution)/shard_map/all_to_all | solution.py:225
  235.2 1.4 reshape_squeeze_reshape.3
  236.7 4.6 %fusion.24 = f32[288,1024]{1,0:T(8,128)} fusion(bf16[288,2048]{1,0:T(8,128)(2,1)S(1)} %reshape_squeeze_reshape.3, bf16[1,2048,1024]{2,1,0:T(8,128)(2,1)} %param.39), kind=kOutput, calls=%fused_computation.33 | convolution fusion | flops 1207959552 | bytes 6553600 | tf_op jit(solution)/shard_map/dot_general | solution.py:234
  242.4 7.9 %fusion.20 = f32[288,2048]{1,0:T(8,128)} fusion(bf16[1,1024,2048]{2,1,0:T(8,128)(2,1)} %param.41, bf16[288,2048]{1,0:T(8,128)(2,1)S(1)} %reshape_squeeze_reshape.3, bf16[1,2048,1024]{2,1,0:T(8,128)(2,1)} %param.40, f32[288,1024]{1,0:T(8,128)} %fusion.24, f32[288]{0:T(512)S(1)} %mul.322), kind=kOutput, calls=%fused_computation.29 | convolution fusion | flops 2417983488 | bytes 13108352 | tf_op jit(solution)/shard_map/dot_general | solution.py:240
  250.4 4.5 %fusion.26 = bf16[288,2048]{1,0:T(8,128)(2,1)} fusion(f32[288,2048]{1,0:T(8,128)} %fusion.20, bf16[128,2048]{1,0:T(8,128)(2,1)} %param.44, bf16[288,2048]{1,0:T(8,128)(2,1)S(1)} %reshape_squeeze_reshape.3, bf16[2048,128]{1,0:T(8,128)(2,1)} %param.43, f32[288,128]{1,0:T(8,128)} %fusion.114, f32[288]{0:T(512)S(1)} %mul.327), kind=kOutput, calls=%fused_computation.36 | convolution fusion | flops 303427584 | bytes 5915776 | tf_op jit(solution)/shard_map/dot_general | solution.py:243
  254.9 2.2 convert_element_type.156
  257.1 25.1 %reduce-scatter.5.cloned.1.call-done = bf16[8,36,512]{2,1,0:T(8,128)(2,1)} async-done(((bf16[8,36,2048]{2,1,0:T(8,128)(2,1)}), bf16[8,36,512]{2,1,0:T(8,128)(2,1)}) %reduce-scatter.5.cloned.1.call-update) | async-done | bytes 294928 | tf_op jit(solution)/shard_map/reduce_scatter | solution.py:248
  282.3 5.5 %all-to-all-start.2 = ((bf16[8,36,512]{2,1,0:T(8,128)(2,1)}), bf16[8,36,512]{2,1,0:T(8,128)(2,1)S(1)}, u32[]{:S(2)}, u32[]{:S(2)}) async-start(bf16[8,36,512]{2,1,0:T(8,128)(2,1)} %reduce-scatter.5.cloned.1.call-done), calls=%async_computation.4 | async-start | bytes 655360 | tf_op jit(solution)/shard_map/all_to_all | solution.py:249
  287.8 10.2 %all-to-all-done.2 = bf16[8,36,512]{2,1,0:T(8,128)(2,1)S(1)} async-done(((bf16[8,36,512]{2,1,0:T(8,128)(2,1)}), bf16[8,36,512]{2,1,0:T(8,128)(2,1)S(1)}, u32[]{:S(2)}, u32[]{:S(2)}) %all-to-all-start.2) | async-done | bytes 294944 | tf_op jit(solution)/shard_map/all_to_all | solution.py:249
  300.2 5.9 %all-reduce.4 = (f32[128]{0:T(128)S(1)}, f32[128]{0:T(128)S(1)}) all-reduce(f32[128]{0:T(128)S(1)} %get-tuple-element.164, f32[128]{0:T(128)S(1)} %get-tuple-element.163), channel_id=1, replica_groups=mesh['sp'=8,'tp'=4] {'tp'}, use_global_device_ids=true, to_apply=%region_22.23 | all-reduce | flops 256 | bytes 2048 | tf_op jit(solution)/shard_map/psum | solution.py:47
  (184 shorter events, 30.3 us)
Async XLA Ops:
  6.5 113.2 %copy-start = (bf16[512,2048]{1,0:T(8,128)(2,1)S(1)}, bf16[512,2048]{1,0:T(8,128)(2,1)}, u32[]{:S(2)}) copy-start(bf16[512,2048]{1,0:T(8,128)(2,1)} %param.34) | copy-start | bytes 6291460
  6.5 3.2 %copy-start.23 = (f32[4]{0:T(128)S(1)}, f32[4]{0:T(128)}, u32[]{:S(2)}) copy-start(f32[4]{0:T(128)} %param.30) | copy-start | bytes 52
  6.5 3.2 %copy-start.20 = (f32[4,128]{1,0:T(4,128)S(1)}, f32[4,128]{1,0:T(4,128)}, u32[]{:S(2)}) copy-start(f32[4,128]{1,0:T(4,128)} %param.29) | copy-start | bytes 6148
  6.5 3.2 %copy-start.19 = (f32[4,128]{1,0:T(4,128)S(1)}, f32[4,128]{1,0:T(4,128)}, u32[]{:S(2)}) copy-start(f32[4,128]{1,0:T(4,128)} %param.31) | copy-start | bytes 6148
  6.5 3.4 %copy-start.21 = (f32[4,128]{1,0:T(4,128)S(1)}, f32[4,128]{1,0:T(4,128)}, u32[]{:S(2)}) copy-start(f32[4,128]{1,0:T(4,128)} %param.28) | copy-start | bytes 6148
  6.5 70.4 %all-gather.6.cloned.1.call-start = ((), (), s32[]{:S(2)}) async-start(), calls=%async_computation.7 | async-start | bytes 1179648 | tf_op jit(solution)/shard_map/all_gather | solution.py:18
  7.5 9.2 %copy-start.14 = (f32[2,64]{1,0:T(2,128)}, f32[2,64]{1,0:T(2,128)S(1)}, u32[]{:S(2)}) copy-start(f32[2,64]{1,0:T(2,128)S(1)} %reshape.263) | copy-start | bytes 1540
  8.4 3.4 %copy-start.12 = (pred[2,64,64]{2,1,0:T(8,128)(4,1)}, pred[2,64,64]{2,1,0:T(8,128)(4,1)S(1)}, u32[]{:S(2)}) copy-start(pred[2,64,64]{2,1,0:T(8,128)(4,1)S(1)} %compare_and_fusion) | copy-start | bytes 24580
  9.6 11.2 %copy-start.2 = (f32[4,128,128]{2,1,0:T(8,128)}, f32[4,128,128]{2,1,0:T(8,128)S(1)}, u32[]{:S(2)}) copy-start(f32[4,128,128]{2,1,0:T(8,128)S(1)} %copy.82) | copy-start | bytes 786436
  14.2 2.7 copy-start.9
  17.0 2.5 copy-start.10
  25.2 1.8 copy-start.3
  25.2 1.9 copy-start.6
  26.6 1.6 copy-start.1
  29.0 1.9 copy-start.3
  29.0 1.9 copy-start.6
  30.4 1.6 copy-start.1
  32.8 1.7 copy-start.15
  32.8 2.8 copy-start.24
  32.8 28.8 %copy-start.16 = (s32[128,2]{0,1:T(2,128)S(1)}, s32[128,2]{0,1:T(2,128)}, u32[]{:S(2)}) copy-start(s32[128,2]{0,1:T(2,128)} %param.37) | copy-start | bytes 3076
  32.9 29.2 %copy-start.8 = (f32[2,4,64,256]{3,2,1,0:T(8,128)S(1)}, f32[2,4,64,256]{3,2,1,0:T(8,128)}, u32[]{:S(2)}) copy-start(f32[2,4,64,256]{3,2,1,0:T(8,128)} %get-tuple-element.123) | copy-start | bytes 1572868
  32.9 29.2 %copy-start.11 = (bf16[128,512]{1,0:T(8,128)(2,1)S(1)}, bf16[128,512]{1,0:T(8,128)(2,1)}, u32[]{:S(2)}) copy-start(bf16[128,512]{1,0:T(8,128)(2,1)} %param.33) | copy-start | bytes 393220
  33.7 84.4 %all-gather.8.cloned.1.call-start = ((), (), s32[]{:S(2)}) async-start(), calls=%async_computation.8 | async-start | bytes 1179648 | tf_op jit(solution)/shard_map/all_gather | solution.py:18
  34.4 143.0 %reduce-scatter.3.cloned.1.call-start = ((), (), s32[]{:S(2)}) async-start(), calls=%async_computation.5 | async-start | bytes 655360 | tf_op jit(solution)/shard_map/reduce_scatter | solution.py:191
  121.0 56.4 %copy-start.5 = (bf16[128,512]{1,0:T(8,128)(2,1)S(1)}, bf16[128,512]{1,0:T(8,128)(2,1)}, u32[]{:S(2)}) copy-start(bf16[128,512]{1,0:T(8,128)(2,1)} %param.35) | copy-start | bytes 393220
  121.0 63.2 %copy-start.17 = (f32[512]{0:T(512)S(1)}, f32[512]{0:T(512)}, u32[]{:S(2)}) copy-start(f32[512]{0:T(512)} %param.36) | copy-start | bytes 6148
  126.0 71.7 %all-to-all-start.1 = ((bf16[8,36,2]{1,2,0:T(2,128)(2,1)}), bf16[8,36,2]{1,2,0:T(2,128)(2,1)S(1)}, u32[]{:S(2)}, u32[]{:S(2)}) async-start(bf16[8,36,2]{1,2,0:T(2,128)(2,1)} %copy.101), calls=%async_computation.2 | async-start | bytes 8192 | tf_op jit(solution)/shard_map/all_to_all | solution.py:226
  197.7 37.5 %all-to-all-start = ((bf16[8,36,2048]{2,1,0:T(8,128)(2,1)}), bf16[8,36,2048]{2,1,0:T(8,128)(2,1)}, u32[]{:S(2)}, u32[]{:S(2)}) async-start(bf16[8,36,2048]{2,1,0:T(8,128)(2,1)} %broadcast_select_fusion), calls=%async_computation.1 | async-start | bytes 2621440 | tf_op jit(solution)/shard_map/all_to_all | solution.py:225
  203.2 79.1 %reduce-scatter.5.cloned.1.call-start = ((), (), s32[]{:S(2)}) async-start(), calls=%async_computation.6 | async-start | bytes 1638400 | tf_op jit(solution)/shard_map/reduce_scatter | solution.py:248
  236.6 4.7 %copy-start.4 = (bf16[2048,128]{1,0:T(8,128)(2,1)S(1)}, bf16[2048,128]{1,0:T(8,128)(2,1)}, u32[]{:S(2)}) copy-start(bf16[2048,128]{1,0:T(8,128)(2,1)} %param.42) | copy-start | bytes 1572868
  282.3 15.7 %all-to-all-start.2 = ((bf16[8,36,512]{2,1,0:T(8,128)(2,1)}), bf16[8,36,512]{2,1,0:T(8,128)(2,1)S(1)}, u32[]{:S(2)}, u32[]{:S(2)}) async-start(bf16[8,36,512]{2,1,0:T(8,128)(2,1)} %reduce-scatter.5.cloned.1.call-done), calls=%async_computation.4 | async-start | bytes 655360 | tf_op jit(solution)/shard_map/all_to_all | solution.py:249
  299.1 7.1 %copy-start.18 = (f32[512]{0:T(512)S(1)}, f32[512]{0:T(512)}, u32[]{:S(2)}) copy-start(f32[512]{0:T(512)} %param.45) | copy-start | bytes 6148
  (4 other events, 4.2 us)
Sparse Core Ops, SparseCore 0:
  33.8 43.0 all-gather.5
  79.0 38.9 all-gather.7
  121.2 56.1 reduce-scatter.2
  257.3 24.9 reduce-scatter.4
where the time goes:
time: 315 us; the launch traced here: 314 us
  waiting for transfers between devices  135 us (43%)
  starting transfers between devices  50.3 us (16%)
  blocking collectives  41.7 us (13%)
  matrix products  34.8 us (11%)
  local copies, waits for them, and re-layouts  25.4 us (8%)
  between operations  14.9 us (5%)
  other arithmetic  11.5 us (4%)
    all_gather x2, waiting for transfers between devices, entering(): lax.all_gather(a.astype(kind), axis)  54.6 us
    all_to_all x1, starting transfers between devices, shards(): lax.all_to_all(slot_info, 'sp', split_axis=0, concat_axis=0, tiled=True)  39.2 us
    all_to_all x1, waiting for transfers between devices, shards(): lax.all_to_all(sent, 'sp', split_axis=0, concat_axis=0, tiled=True)  31.8 us
    reduce_scatter x1, waiting for transfers between devices, shards(): lax.psum_scatter(partials.astype(jnp.bfloat16), 'tp', scatter_dimension=2...  25.1 us
    unnamed x1, blocking collectives  23.1 us
    dot_general x23, matrix products, matmul_high(): return jnp.einsum(form, left, right, precision=HIGH)  15.3 us
    reduce_scatter x1, waiting for transfers between devices, shards(): lax.psum_scatter(partial_proj.astype(jnp.bfloat16), 'tp', scatter_dimensi...  12.2 us
    psum x2, blocking collectives, feature_norm(): lax.psum((jnp.sum(summed, -1), jnp.sum(summed * summed, -1)), 'tp')  11.7 us
  transfers between devices with their start and end apart: 7, of which 6 were waited for; matrix products, arithmetic and copies ran while one was open for 6% of the time, Pallas kernels for 0%

commit v1 on v0

v1 whole, which is shorter than its diff:
```python
import functools

import jax
import jax.numpy as jnp
from jax import lax
from jax.experimental import pallas as pl
from jax.experimental.pallas import tpu as pltpu
from jax.sharding import PartitionSpec as P

DK = 128
DV = 128
BLOCK = 64
DOC_SPAN = 768


HIGH = lax.Precision.HIGHEST
ALPHA = 2.0**0.25
MESH = pl.DeviceIdType.MESH


def vmem_specs(count):
    return [pl.BlockSpec(memory_space=pltpu.VMEM)] * count


def exchange_kernel(axis, n, modes, *refs):
    count = len(modes)
    ins, outs = refs[:count], refs[count : 2 * count]
    send_sem, recv_sem, own_sem = refs[2 * count :]
    me = lax.axis_index(axis)
    barrier = pltpu.get_barrier_semaphore()
    for hop in range(1, n):
        pl.semaphore_signal(
            barrier, inc=1, device_id={axis: lax.rem(me + hop, n)}, device_id_type=MESH
        )

    def span(ref, place, size):
        return ref.at[:, pl.ds(pl.multiple_of(place * size, size), size)]

    def ends(index, target):
        source, landing = ins[index], outs[index]
        if modes[index] == "rows":
            return source.at[target], landing.at[me]
        if modes[index] == "cols":
            return span(source, target, landing.shape[-1]), landing.at[me]
        if modes[index] == "join":
            return source, span(landing, me, source.shape[-1])
        return source, landing.at[me]

    own = []
    for index in range(count):
        source, landing = ends(index, me)
        own.append(pltpu.make_async_copy(source, landing, own_sem.at[index]))
        own[-1].start()
    pl.semaphore_wait(barrier, n - 1)
    sent = []
    for hop in range(1, n):
        target = lax.rem(me + hop, n)
        for index in range(count):
            source, landing = ends(index, target)
            sent.append(
                pltpu.make_async_remote_copy(
                    src_ref=source,
                    dst_ref=landing,
                    send_sem=send_sem.at[index, hop - 1],
                    recv_sem=recv_sem.at[index, hop - 1],
                    device_id={axis: target},
                    device_id_type=MESH,
                )
            )
            sent[-1].start()
    for copy in own + sent:
        copy.wait()


def exchange(arrays, modes, axis, cid):
    n = lax.axis_size(axis)
    count = len(arrays)
    shapes = []
    for array, mode in zip(arrays, modes):
        if mode == "rows":
            shape = array.shape
        elif mode == "cols":
            shape = (n, array.shape[0], array.shape[1] // n)
        elif mode == "join":
            shape = (array.shape[0], array.shape[1] * n)
        else:
            shape = (n,) + array.shape
        shapes.append(jax.ShapeDtypeStruct(shape, array.dtype))
    return pl.pallas_call(
        functools.partial(exchange_kernel, axis, n, modes),
        out_shape=shapes,
        in_specs=vmem_specs(count),
        out_specs=vmem_specs(count),
        scratch_shapes=[
            pltpu.SemaphoreType.DMA((count, n - 1)),
            pltpu.SemaphoreType.DMA((count, n - 1)),
            pltpu.SemaphoreType.DMA((count,)),
        ],
        compiler_params=pltpu.CompilerParams(collective_id=cid, has_side_effects=True),
        name=f"exchange_{axis}_{cid}",
    )(*arrays)


def scan_plan(n, reach):
    hops = [1]
    covered = 1
    if reach > 1 and n > 2:
        hops.append(2)
        covered = 3
        while covered < min(reach, n - 1):
            hops.append(covered)
            covered = 2 * covered
    return hops


def scan_kernel(n, hops, own_ref, out_ref, *scratch):
    rounds = len(hops)
    landed, built = scratch[:rounds], scratch[rounds : 2 * rounds]
    send_sem, recv_sem = scratch[2 * rounds :]
    heads = own_ref.shape[1]
    me = lax.axis_index("sp")
    barrier = pltpu.get_barrier_semaphore()
    for hop in range(1, n):
        pl.semaphore_signal(
            barrier, inc=1, device_id={"sp": lax.rem(me + hop, n)}, device_id_type=MESH
        )
    pl.semaphore_wait(barrier, n - 1)

    def dot(left, right):
        return jnp.dot(left, right, preferred_element_type=jnp.float32)

    def copy_of(index):
        last = index == rounds - 1 and index > 1
        source = own_ref if index == 0 else built[index]
        landing = landed[index]
        if last:
            source, landing = source.at[1], landing.at[1]
        return pltpu.make_async_remote_copy(
            src_ref=source,
            dst_ref=landing,
            send_sem=send_sem.at[index],
            recv_sem=recv_sem.at[index],
            device_id={"sp": lax.rem(me + hops[index], n)},
            device_id_type=MESH,
        )

    window = None
    for index, hop in enumerate(hops):
        copy = copy_of(index)
        last = index == rounds - 1

        @pl.when(me + hop < n)
        def _():
            copy.start()

        @pl.when(me >= hop)
        def _():
            copy.wait_recv()

        @pl.when(me < hop)
        def _():
            landed[index][...] = jnp.zeros_like(landed[index])

        got = landed[index]
        if index == 0:
            if last:
                out_ref[...] = got[1].astype(jnp.float32)
            else:
                later, target = own_ref, built[1]
                for h in range(heads):
                    target[0, h] = dot(later[0, h], got[0, h]).astype(target.dtype)
                    target[1, h] = (
                        dot(later[0, h], got[1, h]) + later[1, h].astype(jnp.float32)
                    ).astype(target.dtype)
            window = got
        else:
            for h in range(heads):
                shift = dot(window[0, h], got[1, h]) + window[1, h].astype(jnp.float32)
                if last:
                    out_ref[h] = shift
                else:
                    target = built[index + 1]
                    target[0, h] = dot(window[0, h], got[0, h]).astype(target.dtype)
                    target[1, h] = shift.astype(target.dtype)
            if not last:
                window = built[index + 1]
    for index, hop in enumerate(hops):

        @pl.when(me + hop < n)
        def _():
            copy_of(index).wait_send()


def entering(summary, reach, cid):
    n = lax.axis_size("sp")
    hops = scan_plan(n, reach)
    block = pltpu.VMEM(summary.shape, summary.dtype)
    return pl.pallas_call(
        functools.partial(scan_kernel, n, hops),
        out_shape=jax.ShapeDtypeStruct(summary.shape[1:], jnp.float32),
        in_specs=vmem_specs(1),
        out_specs=pl.BlockSpec(memory_space=pltpu.VMEM),
        scratch_shapes=[block] * (2 * len(hops))
        + [pltpu.SemaphoreType.DMA((len(hops),)), pltpu.SemaphoreType.DMA((len(hops),))],
        compiler_params=pltpu.CompilerParams(collective_id=cid, has_side_effects=True),
        name="state_scan",
    )(summary)


def unit_rows(array):
    return array * lax.rsqrt(jnp.sum(array * array, -1, keepdims=True) + 1e-06)


def matmul_high(form, left, right):
    return jnp.einsum(form, left, right, precision=HIGH)


def matmul_one(form, left, right):
    return jnp.einsum(
        form,
        left.astype(jnp.bfloat16),
        right.astype(jnp.bfloat16),
        preferred_element_type=jnp.float32,
    )


def feature_norm(summed, gain, cid):
    width = summed.shape[-1] * lax.axis_size("tp")
    own = jnp.stack([jnp.sum(summed, -1), jnp.sum(summed * summed, -1)])
    (parts,) = exchange((own,), ("all",), "tp", cid)
    totals, squares = jnp.sum(parts, 0)
    row_mean = totals / width
    row_var = squares / width - row_mean * row_mean
    return (summed - row_mean[:, None]) * lax.rsqrt(row_var[:, None] + 1e-05) * gain


def block_pass(query_unit, key_unit, write_gate, decay_logarithm, segment, values_in, initial):
    heads_here, blocks, block_len, key_depth = query_unit.shape
    cumulative = jnp.cumsum(decay_logarithm, -1)
    before = jnp.concatenate([segment[:1, 0], segment[:-1, -1]])
    carried = (segment == before[:, None]).astype(jnp.float32)
    same_doc = segment[:, :, None] == segment[:, None, :]
    offsets = jnp.arange(block_len)
    lower_tri = offsets[:, None] >= offsets[None, :]
    strict = offsets[:, None] > offsets[None, :]
    log_gap = cumulative[..., :, None] - cumulative[..., None, :]
    reach_mask = jnp.where(lower_tri & same_doc, jnp.exp(jnp.where(lower_tri, log_gap, 0.0)), 0.0)
    weighted_keys = key_unit * write_gate[..., None]
    coupling = jnp.where(
        strict, matmul_high("hncd,hnsd->hncs", weighted_keys, key_unit) * reach_mask, 0.0
    )
    identity_block = jnp.eye(block_len, dtype=jnp.float32)
    inverse = identity_block - coupling
    nil_power = coupling
    for squaring in range(block_len.bit_length() - 2):
        nil_power = matmul_high("hncs,hnst->hnct", nil_power, nil_power)
        inverse = matmul_high("hncs,hnst->hnct", inverse, identity_block + nil_power)
    growth = jnp.exp(cumulative) * carried
    update = matmul_one("hncs,hnse->hnce", inverse, values_in * write_gate[..., None])
    correction = matmul_one("hncs,hnsd->hncd", inverse, weighted_keys * growth[..., None])
    final_growth = jnp.exp(cumulative[..., -1]) * (segment[:, -1] == before).astype(jnp.float32)
    tail_decay = jnp.exp(cumulative[..., -1:] - cumulative) * (segment == segment[:, -1:]).astype(
        jnp.float32
    )
    tail_keys = key_unit * tail_decay[..., None]
    query_grown = query_unit * growth[..., None]
    local_scores = matmul_one("hncd,hnsd->hncs", query_unit, key_unit) * reach_mask

    def advance(carry_state, inputs):
        grown_query, block_corr, block_update, block_keys, block_scores, block_fade = inputs
        fresh_values = block_update - matmul_one("hcd,hde->hce", block_corr, carry_state)
        next_state = carry_state * block_fade[:, None, None] + matmul_one(
            "hcd,hce->hde", block_keys, fresh_values
        )
        block_out = matmul_one("hcd,hde->hce", grown_query, carry_state) + matmul_one(
            "hcs,hse->hce", block_scores, fresh_values
        )
        return (next_state, block_out)

    inputs = tuple(
        (
            jnp.moveaxis(array, 1, 0)
            for array in (query_grown, correction, update, tail_keys, local_scores, final_growth)
        )
    )
    final_state, outputs = lax.scan(advance, initial, inputs)
    outputs = jnp.moveaxis(outputs, 0, 1).reshape(heads_here, blocks * block_len, -1)
    return (final_state, outputs)


def shards(
    probe_vectors,
    address_vectors,
    content_vectors,
    storage_raw_signal,
    fade_raw_signal,
    channel_fade_exponent,
    extra_fade_amount,
    sequence_label,
    exit_valve_raw_signal,
    final_projection_matrix,
    incoming_rows_matrix,
    initial_rescale_factor,
    specialist_picks,
    picked_specialist_share,
    specialist_valve_matrix,
    specialist_raising_matrix,
    specialist_lowering_matrix,
    common_valve_matrix,
    common_raising_matrix,
    common_lowering_matrix,
    latter_rescale_factor,
):
    tokens_here = probe_vectors.shape[0]
    heads_here = storage_raw_signal.shape[0]
    blocks = tokens_here // BLOCK

    def split_heads(array, width):
        moved = jnp.transpose(
            array.astype(jnp.float32).reshape(tokens_here, heads_here, width), (1, 0, 2)
        )
        return moved.reshape(heads_here, blocks, BLOCK, width)

    query_unit = unit_rows(split_heads(probe_vectors, DK)) * DK ** (-0.5)
    key_unit = unit_rows(split_heads(address_vectors, DK))
    value_rows = split_heads(content_vectors, DV)
    write_gate = jax.nn.sigmoid(storage_raw_signal).reshape(heads_here, blocks, BLOCK)
    decay_logarithm = (
        extra_fade_amount
        - jnp.exp(channel_fade_exponent)[:, None] * jax.nn.softplus(fade_raw_signal)
    ).reshape(heads_here, blocks, BLOCK)
    segment = sequence_label.astype(jnp.float32).reshape(blocks, BLOCK)
    extended = jnp.concatenate(
        [value_rows, jnp.zeros((heads_here, blocks, BLOCK, DK), jnp.float32)], -1
    )
    identity_state = jnp.broadcast_to(jnp.eye(DK, dtype=jnp.float32), (heads_here, DK, DK))
    start_state = jnp.concatenate(
        [jnp.zeros((heads_here, DK, DV), jnp.float32), identity_state], -1
    )
    summary, local_out = block_pass(
        query_unit, key_unit, write_gate, decay_logarithm, segment, extended, start_state
    )
    (edges,) = exchange((sequence_label[None, :],), ("all",), "sp", 0)
    place = lax.axis_index("sp")
    before = lax.dynamic_index_in_dim(edges[:, 0, -1], jnp.maximum(place - 1, 0), 0, False)
    joined = ((before == sequence_label[0]) & (place > 0)).astype(jnp.float32)
    reach = -(-(DOC_SPAN - 1) // tokens_here)
    own = jnp.stack([summary[..., DV:] * joined, summary[..., :DV]]).astype(jnp.bfloat16)
    incoming = entering(own, reach, 1) * joined
    memory_layer_result = local_out[..., :DV] + matmul_one(
        "hcd,hde->hce", local_out[..., DV:], incoming
    )
    scaled = memory_layer_result * lax.rsqrt(
        jnp.mean(memory_layer_result * memory_layer_result, -1, keepdims=True) + 1e-06
    )
    token_major = jnp.transpose(scaled, (1, 0, 2)).reshape(tokens_here, heads_here * DV)
    heads_out = (token_major * jax.nn.silu(exit_valve_raw_signal.astype(jnp.float32))).astype(
        jnp.bfloat16
    )
    partial_proj = jnp.dot(heads_out, final_projection_matrix, preferred_element_type=jnp.float32)
    (shares,) = exchange((partial_proj.astype(jnp.bfloat16),), ("cols",), "tp", 2)
    projected = jnp.sum(shares.astype(jnp.float32), 0)
    middle = feature_norm(
        ALPHA * incoming_rows_matrix.astype(jnp.float32) + projected, initial_rescale_factor, 3
    ).astype(jnp.bfloat16)
    top = specialist_picks.shape[1]
    local_experts = specialist_valve_matrix.shape[0]
    experts_all = local_experts * lax.axis_size("sp")
    capacity = max(2, 9 * tokens_here * top // (8 * experts_all))
    picks = tokens_here * top
    flat_routes = specialist_picks.reshape(picks)
    one_hot = (flat_routes[:, None] == jnp.arange(experts_all, dtype=jnp.int32)[None, :]).astype(
        jnp.int32
    )
    rank_in = jnp.sum(jnp.cumsum(one_hot, 0) * one_hot, 1) - 1
    slot_of = flat_routes * capacity + rank_in
    slots = experts_all * capacity
    slot_table = slot_of.reshape(tokens_here, top)
    matches = [
        jnp.arange(slots, dtype=jnp.int32)[:, None] == slot_table[None, :, j] for j in range(top)
    ]
    pick = functools.reduce(jnp.logical_or, matches).astype(jnp.bfloat16)
    slot_weight = sum(
        jnp.sum(
            jnp.where(matches[j], picked_specialist_share[None, :, j].astype(jnp.float32), 0.0), 1
        )
        for j in range(top)
    )
    slot_shared = jnp.any(matches[0], 1).astype(jnp.float32)
    slot_info = jnp.stack([slot_weight, slot_shared]).astype(jnp.bfloat16)
    slot_info = jnp.moveaxis(slot_info.reshape(2, experts_all, capacity), 0, 1)
    sp_size = lax.axis_size("sp")
    slot_count = capacity * local_experts
    sent = jnp.dot(pick, middle, preferred_element_type=jnp.float32).astype(jnp.bfloat16)
    arrived, info = exchange(
        (sent.reshape(sp_size, slot_count, -1), slot_info.reshape(sp_size, local_experts * 2, capacity)),
        ("rows", "rows"),
        "sp",
        5,
    )
    sources = sp_size
    (inputs_e,) = exchange((arrived.reshape(sources * slot_count, -1),), ("join",), "tp", 6)
    info = info.astype(jnp.float32)
    weight_e = info[:, 0].reshape(-1, 1)
    shared_e = info[:, 1].reshape(-1, 1)
    gate_e = jnp.dot(inputs_e, specialist_valve_matrix[0], preferred_element_type=jnp.float32)
    up_e = jnp.dot(inputs_e, specialist_raising_matrix[0], preferred_element_type=jnp.float32)
    hidden_e = (jax.nn.silu(gate_e) * up_e * weight_e).astype(jnp.bfloat16)
    shared_g = jnp.dot(inputs_e, common_valve_matrix, preferred_element_type=jnp.float32)
    shared_u = jnp.dot(inputs_e, common_raising_matrix, preferred_element_type=jnp.float32)
    shared_hidden = (jax.nn.silu(shared_g) * shared_u * shared_e).astype(jnp.bfloat16)
    partial_out = jnp.dot(
        hidden_e, specialist_lowering_matrix[0], preferred_element_type=jnp.float32
    )
    partial_out = partial_out + jnp.dot(
        shared_hidden, common_lowering_matrix, preferred_element_type=jnp.float32
    )
    (pieces,) = exchange((partial_out.astype(jnp.bfloat16),), ("cols",), "tp", 7)
    summed = jnp.sum(pieces.astype(jnp.float32), 0).astype(jnp.bfloat16)
    (returned,) = exchange((summed.reshape(sources, slot_count, -1),), ("rows",), "sp", 8)
    mixture = lax.dot_general(
        pick,
        returned.reshape(slots, -1),
        (((0,), (0,)), ((), ())),
        preferred_element_type=jnp.float32,
    )
    second_sum = ALPHA * middle.astype(jnp.float32) + mixture
    return feature_norm(second_sum, latter_rescale_factor, 4).astype(jnp.bfloat16)


def solution(mesh):
    placed = (
        P("sp", "tp"),
        P("sp", "tp"),
        P("sp", "tp"),
        P("tp", "sp"),
        P("tp", "sp"),
        P("tp"),
        P("tp", "sp"),
        P("sp"),
        P("sp", "tp"),
        P("tp", None),
        P("sp", "tp"),
        P("tp"),
        P("sp", None),
        P("sp", None),
        P("sp", None, "tp"),
        P("sp", None, "tp"),
        P("sp", "tp", None),
        P(None, "tp"),
        P(None, "tp"),
        P("tp", None),
        P("tp"),
    )
    return jax.shard_map(
        shards, mesh=mesh, in_specs=placed, out_specs=P("sp", "tp"), check_vma=False
    )
```

time: 315 us -> 177 us (0.56)
  waiting for transfers between devices: 135 us -> 0 us
  Pallas kernels: 0 us -> 112 us
  starting transfers between devices: 50.3 us -> 0 us
  blocking collectives: 41.7 us -> 0 us
  between operations: 14.9 us -> 1.43 us
  local copies, waits for them, and re-layouts: 25.4 us -> 16.6 us
  matrix products: 34.8 us -> 30.7 us
  other arithmetic: 11.5 us -> 15 us
    pallas_call x0 -> x9, Pallas kernels: none -> 112 us  [the longest x8 98.9 us: exchange(): pl.pallas_call(functools.partial(exchange_kernel, axis, n, modes), out_sh...]
    all_gather x2 -> x0, waiting for transfers between devices: 54.6 us -> none  [entering(): lax.all_gather(a.astype(kind), axis)]
    all_to_all x3 -> x0, starting transfers between devices: 50.2 us -> none  [the longest x1 39.2 us: shards(): lax.all_to_all(slot_info, 'sp', split_axis=0, concat_axis=0, tiled=True)]
    all_to_all x3 -> x0, waiting for transfers between devices: 41.9 us -> none  [the longest x1 31.8 us: shards(): lax.all_to_all(sent, 'sp', split_axis=0, concat_axis=0, tiled=True)]
    reduce_scatter x2 -> x0, waiting for transfers between devices: 37.3 us -> none  [the longest x1 25.1 us: shards(): lax.psum_scatter(partials.astype(jnp.bfloat16), 'tp', scatter_dimension=2...]
    unnamed x1 -> x0, blocking collectives: 23.1 us -> none
    psum x2 -> x0, blocking collectives: 11.7 us -> none  [feature_norm(): lax.psum((jnp.sum(summed, -1), jnp.sum(summed * summed, -1)), 'tp')]
    dot_general x23 -> x11, matrix products: 15.3 us -> 4.62 us  [matmul_high(): return jnp.einsum(form, left, right, precision=HIGH)]
  transfers between devices with their start and end apart: 7 -> 0, of which waited for: 6 -> 0; matrix products, arithmetic and copies ran while one was open for 6% -> 0% of each run, Pallas kernels for 0% -> 0%
where the time goes in v1:
time: 177 us; the launch traced here: 176 us
  Pallas kernels  112 us (63%)
  matrix products  30.7 us (17%)
  local copies, waits for them, and re-layouts  16.6 us (9%)
  other arithmetic  15 us (8%)
    pallas_call x8, Pallas kernels, exchange(): pl.pallas_call(functools.partial(exchange_kernel, axis, n, modes), out_sh...  98.9 us
    pallas_call x1, Pallas kernels, entering(): pl.pallas_call(functools.partial(scan_kernel, n, hops), out_shape=jax.Sha...  13.3 us
    dot_general x1, matrix products, shards(): jnp.dot(hidden_e, specialist_lowering_matrix[0], preferred_element_type=j...  7.94 us
    dot_general x12, matrix products, matmul_one(): jnp.einsum(form, left.astype(jnp.bfloat16), right.astype(jnp.bfloat16), p...  5.34 us
    dot_general x1, matrix products, shards(): jnp.dot(inputs_e, specialist_valve_matrix[0], preferred_element_type=jnp....  5.04 us
    dot_general x11, matrix products, matmul_high(): return jnp.einsum(form, left, right, precision=HIGH)  4.62 us
    dot_general x1, matrix products, shards(): jnp.dot(shared_hidden, common_lowering_matrix, preferred_element_type=jnp...  4.44 us

profile of v1, /device:TPU:0, one launch (start us, length us, event | category | flops | bytes accessed | tf_op | source)
XLA Modules:
  0.0 176.2 jit_solution(5891783440414078564)
XLA Ops:
  0.0 0.8 convert_element_type.190
  1.0 1.0 copy.108
  2.5 0.9 reduce_window_sum.26
  9.1 1.8 %compare_convert_fusion.2 = (f32[2]{0:T(128)}, f32[2]{0:T(128)S(1)}) fusion(f32[2]{0:T(128)S(1)} %slice_reduce_fusion.3, f32[1]{0:T(128)} %bitcast.9, f32[1]{0:T(128)} %bitcast.8), kind=kLoop, calls=%fused_computation.158 | loop fusion | flops 6 | bytes 32 | tf_op jit(solution)/shard_map/convert_element_type | solution.py:261
  12.5 1.0 convolution_bitcast_fusion
  13.7 0.8 copy.113
  14.6 1.3 multiply_bitcast_fusion.1
  15.9 1.9 %fusion.36 = bf16[2,4,64,64]{3,2,0,1:T(8,128)(2,1)} fusion(f32[4,2,64,128]{3,2,1,0:T(8,128)S(1)} %bitcast.216, f32[4,2,64,128]{3,2,1,0:T(8,128)} %bitcast.218, f32[2,4,64]{2,0,1:T(2,128)S(1)} %bitcast.222, f32[4,2,64]{2,1,0:T(2,128)S(1)} %rsqrt.49, f32[4,2,64]{2,1,0:T(2,128)S(1)} %copy-done.13, pred[64,64]{1,0:T(8,128)(4,1)S(1)} %get-tuple-element.146, ...), kind=kOutput, calls=%fused_computation.43 | convolution fusion | flops 8880128 | bytes 608256 | tf_op jit(solution)/shard_map/hncd,hnsd->hncs/dot_general | solution.py:219
  18.0 4.9 %while.12 = (s32[]{:T(128)}, f32[4,128,256]{2,1,0:T(8,128)S(1)}, f32[2,4,64,256]{3,2,1,0:T(8,128)}, f32[2,4]{1,0:T(2,128)S(1)}, bf16[2,4,64,128]{3,2,0,1:T(8,128...) while((s32[]{:T(128)}, f32[4,128,256]{2,1,0:T(8,128)S(1)}, ...), condition=%wide.region_4.5_spmd, body=%wide.region_3.4_spmd.sunk | while | flops 59441152 | bytes 8260325 | solution.py:286
  23.0 9.6 %exchange_sp_0.1 = s32[8,1,128]{2,1,0:T(1,128)} custom-call(s32[1,128]{1,0:T(1,128)} %bitcast.226), custom_call_target="tpu_custom_call" | custom-call | tf_op jit(solution)/shard_map/exchange_sp_0/pallas_call | solution.py:89
  35.3 13.3 %state_scan.1 = f32[4,128,128]{2,1,0:T(8,128)} custom-call(bf16[2,4,128,128]{3,2,1,0:T(8,128)(2,1)} %pad_maximum_fusion.own_ref), custom_call_target="tpu_custom_call" | custom-call | tf_op jit(solution)/shard_map/state_scan/pallas_call | solution.py:198
  48.8 0.9 copy-done.2
  50.4 1.3 convolution_convert_fusion.refs_0_
  51.7 9.6 %exchange_tp_2.1 = bf16[4,128,512]{2,1,0:T(8,128)(2,1)} custom-call(bf16[128,2048]{1,0:T(8,128)(2,1)} %convolution_convert_fusion.refs_0_), custom_call_target="tpu_custom_call" | custom-call | tf_op jit(solution)/shard_map/exchange_tp_2/pallas_call | solution.py:89
  61.3 1.1 convert_reduce_fusion
  63.2 5.3 %exchange_tp_3.1 = f32[4,2,128]{2,1,0:T(2,128)} custom-call(f32[2,128]{1,0:T(2,128)} %pad_maximum_fusion.1.refs_0_), custom_call_target="tpu_custom_call" | custom-call | tf_op jit(solution)/shard_map/exchange_tp_3/pallas_call | solution.py:89
  71.2 0.8 reshape.316.refs_0_
  73.1 21.8 %exchange_sp_5.1 = (bf16[8,36,512]{2,1,0:T(8,128)(2,1)}, bf16[8,2,36]{2,1,0:T(2,128)(2,1)}) custom-call(bf16[8,36,512]{2,1,0:T(8,128)(2,1)} %reshape.316.refs_0_, bf16[8,2,36]{2,1,0:T(2,128)(2,1)} %maximum_bitcast_fusion.refs_1_), custom_call_target="tpu_custom_call" | custom-call | tf_op jit(solution)/shard_map/exchange_sp_5/pallas_call | solution.py:89
  95.0 1.7 reshape.317.refs_0_
  96.7 16.7 %exchange_tp_6.1 = bf16[288,2048]{1,0:T(8,128)(2,1)} custom-call(bf16[288,512]{1,0:T(8,128)(2,1)} %reshape.317.refs_0_), custom_call_target="tpu_custom_call" | custom-call | tf_op jit(solution)/shard_map/exchange_tp_6/pallas_call | solution.py:89
  113.4 5.0 %fusion.23 = f32[288,1024]{1,0:T(8,128)} fusion(bf16[288,2048]{1,0:T(8,128)(2,1)} %exchange_tp_6.1, bf16[1,2048,1024]{2,1,0:T(8,128)(2,1)} %param.37), kind=kOutput, calls=%fused_computation.27 | convolution fusion | flops 1207959552 | bytes 6553600 | tf_op jit(solution)/shard_map/dot_general | solution.py:406
  119.2 7.9 %fusion.19 = f32[288,2048]{1,0:T(8,128)} fusion(bf16[1,1024,2048]{2,1,0:T(8,128)(2,1)} %param.39, bf16[288,2048]{1,0:T(8,128)(2,1)S(1)} %copy-done.1, bf16[1,2048,1024]{2,1,0:T(8,128)(2,1)} %param.38, f32[288,1024]{1,0:T(8,128)} %fusion.23, f32[288]{0:T(512)S(1)} %mul.315), kind=kOutput, calls=%fused_computation.23 | convolution fusion | flops 2417983488 | bytes 13108352 | tf_op jit(solution)/shard_map/dot_general | solution.py:412
  127.1 1.5 fusion.114
  128.7 1.4 mul.320
  130.0 4.4 %fusion.25.refs_0_ = bf16[288,2048]{1,0:T(8,128)(2,1)} fusion(f32[288,2048]{1,0:T(8,128)} %fusion.19, bf16[128,2048]{1,0:T(8,128)(2,1)} %param.42, bf16[288,2048]{1,0:T(8,128)(2,1)S(1)} %copy-done.1, bf16[2048,128]{1,0:T(8,128)(2,1)} %param.41, f32[288,128]{1,0:T(8,128)S(1)} %fusion.114, f32[288]{0:T(512)} %mul.320), kind=kOutput, calls=%fused_computation.30 | convolution fusion | flops 303427584 | bytes 5915776 | tf_op jit(solution)/shard_map/dot_general | solution.py:415
  134.5 17.4 %exchange_tp_7.1 = bf16[4,288,512]{2,1,0:T(8,128)(2,1)} custom-call(bf16[288,2048]{1,0:T(8,128)(2,1)} %fusion.25.refs_0_), custom_call_target="tpu_custom_call" | custom-call | tf_op jit(solution)/shard_map/exchange_tp_7/pallas_call | solution.py:89
  151.8 1.5 reduce_sum.139
  153.4 0.8 reshape.318.refs_0_
  154.2 13.6 %exchange_sp_8.1 = bf16[8,36,512]{2,1,0:T(8,128)(2,1)} custom-call(bf16[8,36,512]{2,1,0:T(8,128)(2,1)} %reshape.318.refs_0_), custom_call_target="tpu_custom_call" | custom-call | tf_op jit(solution)/shard_map/exchange_sp_8/pallas_call | solution.py:89
  167.8 1.0 reshape.319
  169.8 4.9 %exchange_tp_4.1 = f32[4,2,128]{2,1,0:T(2,128)} custom-call(f32[2,128]{1,0:T(2,128)} %pad_maximum_fusion.2.refs_0_), custom_call_target="tpu_custom_call" | custom-call | tf_op jit(solution)/shard_map/exchange_tp_4/pallas_call | solution.py:89
  175.4 0.8 multiply_convert_fusion.2
  (177 shorter events, 22.5 us)
Async XLA Ops:
  0.0 50.4 %copy-start = (bf16[512,2048]{1,0:T(8,128)(2,1)S(1)}, bf16[512,2048]{1,0:T(8,128)(2,1)}, u32[]{:S(2)}) copy-start(bf16[512,2048]{1,0:T(8,128)(2,1)} %param.32) | copy-start | bytes 6291460
  0.0 2.4 %copy-start.33 = (f32[4]{0:T(128)S(1)}, f32[4]{0:T(128)}, u32[]{:S(2)}) copy-start(f32[4]{0:T(128)} %param.28) | copy-start | bytes 52
  0.0 2.4 %copy-start.29 = (f32[4,128]{1,0:T(4,128)S(1)}, f32[4,128]{1,0:T(4,128)}, u32[]{:S(2)}) copy-start(f32[4,128]{1,0:T(4,128)} %param.27) | copy-start | bytes 6148
  0.0 2.4 %copy-start.28 = (f32[4,128]{1,0:T(4,128)S(1)}, f32[4,128]{1,0:T(4,128)}, u32[]{:S(2)}) copy-start(f32[4,128]{1,0:T(4,128)} %param.29) | copy-start | bytes 6148
  0.0 3.5 %copy-start.30 = (f32[4,128]{1,0:T(4,128)S(1)}, f32[4,128]{1,0:T(4,128)}, u32[]{:S(2)}) copy-start(f32[4,128]{1,0:T(4,128)} %param.26) | copy-start | bytes 6148
  1.0 3.3 %copy-start.15 = (pred[2,64,64]{2,1,0:T(8,128)(4,1)}, pred[2,64,64]{2,1,0:T(8,128)(4,1)S(1)}, u32[]{:S(2)}) copy-start(pred[2,64,64]{2,1,0:T(8,128)(4,1)S(1)} %compare_and_fusion) | copy-start | bytes 24580
  2.4 9.6 %copy-start.12 = (f32[4,2,64]{2,1,0:T(2,128)}, f32[4,2,64]{2,1,0:T(2,128)S(1)}, u32[]{:S(2)}) copy-start(f32[4,2,64]{2,1,0:T(2,128)S(1)} %rsqrt.47) | copy-start | bytes 6148
  3.6 8.4 %copy-start.14 = (f32[4,2,64]{2,1,0:T(2,128)}, f32[4,2,64]{2,1,0:T(2,128)S(1)}, u32[]{:S(2)}) copy-start(f32[4,2,64]{2,1,0:T(2,128)S(1)} %mul.275) | copy-start | bytes 6148
  7.5 4.9 %copy-start.8 = (bf16[128,512]{1,0:T(8,128)(2,1)S(1)}, bf16[128,512]{1,0:T(8,128)(2,1)}, u32[]{:S(2)}) copy-start(bf16[128,512]{1,0:T(8,128)(2,1)} %param.25) | copy-start | bytes 393220
  8.3 5.1 %copy-start.9 = (bf16[128,512]{1,0:T(8,128)(2,1)S(1)}, bf16[128,512]{1,0:T(8,128)(2,1)}, u32[]{:S(2)}) copy-start(bf16[128,512]{1,0:T(8,128)(2,1)} %param.23) | copy-start | bytes 393220
  12.5 2.2 %copy-start.11 = (f32[4,2,64]{2,1,0:T(2,128)S(1)}, f32[4,2,64]{2,1,0:T(2,128)}, u32[]{:S(2)}) copy-start(f32[4,2,64]{2,1,0:T(2,128)} %get-tuple-element.132) | copy-start | bytes 6148
  12.5 2.1 %copy-start.13 = (f32[4,2,64]{2,1,0:T(2,128)S(1)}, f32[4,2,64]{2,1,0:T(2,128)}, u32[]{:S(2)}) copy-start(f32[4,2,64]{2,1,0:T(2,128)} %copy-done.12) | copy-start | bytes 6148
  13.5 2.5 %copy-start.16 = (pred[2,64,64]{2,1,0:T(8,128)(4,1)S(1)}, pred[2,64,64]{2,1,0:T(8,128)(4,1)}, u32[]{:S(2)}) copy-start(pred[2,64,64]{2,1,0:T(8,128)(4,1)} %copy-done.15) | copy-start | bytes 24580
  13.6 4.2 %copy-start.18 = (f32[4,2,1]{0,1,2:T(2,128)S(1)}, f32[4,2,1]{0,1,2:T(2,128)}, u32[]{:S(2)}) copy-start(f32[4,2,1]{0,1,2:T(2,128)} %copy-done.17) | copy-start | bytes 100
  13.6 4.2 %copy-start.27 = (f32[2]{0:T(128)S(1)}, f32[2]{0:T(128)}, u32[]{:S(2)}) copy-start(f32[2]{0:T(128)} %get-tuple-element.130) | copy-start | bytes 28
  18.0 15.8 %copy-start.32 = (s32[128]{0:T(128)S(1)}, s32[128]{0:T(128)}, u32[]{:S(2)}) copy-start(s32[128]{0:T(128)} %param.30) | copy-start | bytes 1540
  18.1 1.1 copy-start.4
  20.5 1.1 copy-start.4
  23.0 25.7 %copy-start.6 = (f32[2,4,64,256]{3,2,1,0:T(8,128)S(1)}, f32[2,4,64,256]{3,2,1,0:T(8,128)}, u32[]{:S(2)}) copy-start(f32[2,4,64,256]{3,2,1,0:T(8,128)} %get-tuple-element.55) | copy-start | bytes 1572868
  48.7 1.0 copy-start.2
  48.7 1.5 copy-start.10
  51.7 10.8 %copy-start.7 = (bf16[128,512]{1,0:T(8,128)(2,1)S(1)}, bf16[128,512]{1,0:T(8,128)(2,1)}, u32[]{:S(2)}) copy-start(bf16[128,512]{1,0:T(8,128)(2,1)} %param.33) | copy-start | bytes 393220
  51.7 17.5 %copy-start.25 = (f32[512]{0:T(512)S(1)}, f32[512]{0:T(512)}, u32[]{:S(2)}) copy-start(f32[512]{0:T(512)} %param.34) | copy-start | bytes 6148
  51.7 17.6 %copy-start.23 = (s32[128,2]{0,1:T(2,128)S(1)}, s32[128,2]{0,1:T(2,128)}, u32[]{:S(2)}) copy-start(s32[128,2]{0,1:T(2,128)} %param.35) | copy-start | bytes 3076
  62.5 9.5 %copy-start.31 = (bf16[128,2]{0,1:T(2,128)(2,1)S(1)}, bf16[128,2]{0,1:T(2,128)(2,1)}, u32[]{:S(2)}) copy-start(bf16[128,2]{0,1:T(2,128)(2,1)} %param.36) | copy-start | bytes 1540
  70.9 25.8 %copy-start.19 = (s32[128]{0:T(128)}, s32[128]{0:T(128)S(1)}, u32[]{:S(2)}) copy-start(s32[128]{0:T(128)S(1)} %get-tuple-element.133) | copy-start | bytes 1540
  70.9 25.8 %copy-start.21 = (s32[128]{0:T(128)}, s32[128]{0:T(128)S(1)}, u32[]{:S(2)}) copy-start(s32[128]{0:T(128)S(1)} %get-tuple-element.134) | copy-start | bytes 1540
  113.4 5.1 %copy-start.24 = (bf16[8,2,36]{2,1,0:T(2,128)(2,1)S(1)}, bf16[8,2,36]{2,1,0:T(2,128)(2,1)}, u32[]{:S(2)}) copy-start(bf16[8,2,36]{2,1,0:T(2,128)(2,1)} %get-tuple-element.58) | copy-start | bytes 3460
  113.4 5.8 %copy-start.1 = (bf16[288,2048]{1,0:T(8,128)(2,1)S(1)}, bf16[288,2048]{1,0:T(8,128)(2,1)}, u32[]{:S(2)}) copy-start(bf16[288,2048]{1,0:T(8,128)(2,1)} %exchange_tp_6.1) | copy-start | bytes 3538948
  153.4 15.4 %copy-start.20 = (s32[128]{0:T(128)S(1)}, s32[128]{0:T(128)}, u32[]{:S(2)}) copy-start(s32[128]{0:T(128)} %copy-done.19) | copy-start | bytes 1540
  153.4 15.4 %copy-start.22 = (s32[128]{0:T(128)S(1)}, s32[128]{0:T(128)}, u32[]{:S(2)}) copy-start(s32[128]{0:T(128)} %copy-done.21) | copy-start | bytes 1540
  153.4 22.0 %copy-start.26 = (f32[512]{0:T(512)S(1)}, f32[512]{0:T(512)}, u32[]{:S(2)}) copy-start(f32[512]{0:T(512)} %param.43) | copy-start | bytes 6148
  (5 other events, 4.2 us)

commit v2 on v1

--- a/solution.py
+++ b/solution.py
@@ -224,14 +224,270 @@
     )
 
 
-def feature_norm(summed, gain, cid):
-    width = summed.shape[-1] * lax.axis_size("tp")
-    own = jnp.stack([jnp.sum(summed, -1), jnp.sum(summed * summed, -1)])
-    (parts,) = exchange((own,), ("all",), "tp", cid)
-    totals, squares = jnp.sum(parts, 0)
-    row_mean = totals / width
-    row_var = squares / width - row_mean * row_mean
-    return (summed - row_mean[:, None]) * lax.rsqrt(row_var[:, None] + 1e-05) * gain
+def row_stats(array):
+    lane = lax.broadcasted_iota(jnp.int32, (array.shape[0], 128), 1)
+    total = jnp.sum(array, -1, keepdims=True)
+    square = jnp.sum(array * array, -1, keepdims=True)
+    return jnp.where(lane == 0, total, jnp.where(lane == 1, square, 0.0)).T[:8]
+
+
+def columns_of(rows):
+    return jnp.concatenate([rows] * (128 // rows.shape[0]), 0).T
+
+
+def layer_kernel(
+    ns, nt, cap, pad, heads_ref, wo_ref, rows_ref, gain_ref, last_gain_ref, pick_ref, pick_t_ref,
+    info_ref, wv_hbm, wr_hbm, wd_hbm, cv_hbm, cr_hbm, cd_hbm, out_ref,
+    wv_ref, wr_ref, wd_ref, cv_ref, cr_ref, cd_ref, weight_sem,
+    head_out, head_in, head_yout, head_yin, head_sem,
+    stat_own, stat_in, stat_sem,
+    sbuf, gathered, infos, sp_sem, info_sem, y_sem, pair_sem,
+    inputs, hidden, shared, side, part_out, part_in, part_yout, part_yin, part_sem,
+    back_out, back_in, back_sem, returned,
+):
+    sp, tp = lax.axis_index("sp"), lax.axis_index("tp")
+    chips = nt // 2
+    chip, core = tp // 2, lax.rem(tp, 2)
+    partner = tp + 1 - 2 * core
+    width = out_ref.shape[-1]
+    loads = [
+        pltpu.make_async_copy(source, target, weight_sem.at[i])
+        for i, (source, target) in enumerate(
+            (
+                (cv_hbm, cv_ref),
+                (cr_hbm, cr_ref),
+                (wv_hbm.at[0], wv_ref),
+                (wr_hbm.at[0], wr_ref),
+                (cd_hbm, cd_ref),
+                (wd_hbm.at[0], wd_ref),
+            )
+        )
+    ]
+    for load in loads:
+        load.start()
+    barrier = pltpu.get_barrier_semaphore()
+    for hop in range(1, ns):
+        pl.semaphore_signal(
+            barrier, inc=1, device_id={"sp": lax.rem(sp + hop, ns)}, device_id_type=MESH
+        )
+    for hop in range(1, nt):
+        pl.semaphore_signal(
+            barrier, inc=1, device_id={"tp": lax.rem(tp + hop, nt)}, device_id_type=MESH
+        )
+    inputs[...] = jnp.zeros_like(inputs)
+    returned[...] = jnp.zeros_like(returned)
+    pl.semaphore_wait(barrier, ns - 1 + nt - 1)
+    waits = []
+
+    def send(source, target, sems, place, where):
+        copy = pltpu.make_async_remote_copy(
+            src_ref=source,
+            dst_ref=target,
+            send_sem=sems.at[(0,) + place],
+            recv_sem=sems.at[(1,) + place],
+            device_id=where,
+            device_id_type=MESH,
+        )
+        copy.start()
+        waits.append(copy)
+        return copy
+
+    def dot(left, right):
+        return jnp.dot(left, right, preferred_element_type=jnp.float32)
+
+    def sum_over_tp(block, put, take, out, landed, yout, yin, sems):
+        order = list(range(1, chips)) + [0]
+        pairs = {}
+        for k in order:
+            put(out, k, block(2 * lax.rem(chip + k, chips) + 1 - core))
+            pairs[k] = send(out.at[k], landed.at[k], sems, (k,), {"tp": partner})
+        across = []
+        for k in order:
+            there = 2 * lax.rem(chip + k, chips) + core
+            value = block(there)
+            pairs[k].wait_recv()
+            value = value + take(landed, k)
+            if k:
+                put(yout, k - 1, value)
+                across.append(
+                    send(yout.at[k - 1], yin.at[k - 1], sems, (chips + k - 1,), {"tp": there})
+                )
+        for k, copy in enumerate(across):
+            copy.wait_recv()
+            value = value + take(yin, k)
+        return value
+
+    def normed(summed, gain, index):
+        stat_own[index] = row_stats(summed)
+        copies = []
+        for hop in range(1, nt):
+            copies.append(
+                send(
+                    stat_own.at[index],
+                    stat_in.at[index, hop - 1],
+                    stat_sem,
+                    (index, hop - 1),
+                    {"tp": lax.rem(tp + hop, nt)},
+                )
+            )
+        total = stat_own[index]
+        for hop in range(1, nt):
+            copies[hop - 1].wait_recv()
+            total = total + stat_in[index, hop - 1]
+        total = columns_of(total / (width * nt))
+        mean, square = total[:, 0:1], total[:, 1:2]
+        return (summed - mean) * lax.rsqrt(square - mean * mean + 1e-05) * gain
+
+    def head_block(t):
+        start = pl.multiple_of(t * width, width)
+        return dot(heads_ref[...], wo_ref[:, pl.ds(start, width)])
+
+    def put_plain(ref, k, value):
+        ref[k] = value.astype(ref.dtype)
+
+    def take_plain(ref, k):
+        return ref[k].astype(jnp.float32)
+
+    projected = sum_over_tp(
+        head_block, put_plain, take_plain, head_out, head_in, head_yout, head_yin, head_sem
+    )
+    middle = normed(
+        ALPHA * rows_ref[...].astype(jnp.float32) + projected, gain_ref[...], 0
+    ).astype(jnp.bfloat16)
+    picked = dot(pick_ref[...], middle).astype(jnp.bfloat16)
+    for e in range(ns):
+        sbuf[e] = picked[e * pad : e * pad + cap]
+    arrivals, notes = [], []
+    for hop in range(1, ns):
+        to = lax.rem(sp + hop, ns)
+        notes.append(
+            send(info_ref.at[to], infos.at[sp], info_sem, (hop - 1,), {"sp": to})
+        )
+        arrivals.append(
+            send(sbuf.at[to], gathered.at[tp, sp], sp_sem, (hop - 1,), {"sp": to})
+        )
+    gathered[tp, sp] = sbuf[sp]
+    infos[sp] = info_ref[sp]
+    forward, across = [], []
+    for hop in range(ns):
+        source = lax.rem(sp - hop + ns, ns)
+        if hop:
+            arrivals[hop - 1].wait_recv()
+        mine = gathered.at[tp, source]
+        for k in range(1, chips):
+            across.append(
+                (
+                    hop,
+                    k,
+                    send(
+                        mine, mine, y_sem, (hop, k - 1),
+                        {"tp": 2 * lax.rem(chip + k, chips) + core},
+                    ),
+                )
+            )
+        forward.append(send(mine, mine, pair_sem, (hop, 0), {"tp": partner}))
+    for hop, k, copy in across:
+        copy.wait_recv()
+        source = lax.rem(sp - hop + ns, ns)
+        theirs = gathered.at[2 * lax.rem(chip - k + chips, chips) + core, source]
+        forward.append(send(theirs, theirs, pair_sem, (hop, k), {"tp": partner}))
+    for copy in forward + notes:
+        copy.wait_recv()
+    for j in range(ns):
+        for t in range(nt):
+            inputs[j * pad : j * pad + cap, t * width : (t + 1) * width] = gathered[t, j]
+        note = columns_of(infos[j])[:pad]
+        side[j * pad : (j + 1) * pad] = note
+    weight_e, shared_e = side[:, 0:1], side[:, 1:2]
+    for load in loads[:4]:
+        load.wait()
+    shared[...] = (
+        jax.nn.silu(dot(inputs[...], cv_ref[...])) * dot(inputs[...], cr_ref[...]) * shared_e
+    ).astype(jnp.bfloat16)
+    units = hidden.shape[1]
+    tile = 256 if units % 256 == 0 else 128
+
+    @pl.loop(0, units // tile)
+    def _(i):
+        cols = pl.ds(pl.multiple_of(i * tile, tile), tile)
+        gate = dot(inputs[...], wv_ref[:, cols])
+        up = dot(inputs[...], wr_ref[:, cols])
+        hidden[:, cols] = (jax.nn.silu(gate) * up * weight_e).astype(jnp.bfloat16)
+
+    for load in loads[4:]:
+        load.wait()
+
+    def part_block(t):
+        cols = pl.ds(pl.multiple_of(t * width, width), width)
+        return dot(hidden[...], wd_ref[:, cols]) + dot(shared[...], cd_ref[:, cols])
+
+    def put_groups(ref, k, value):
+        value = value.astype(ref.dtype)
+        for j in range(ns):
+            ref[k, j] = value[j * pad : j * pad + cap]
+
+    def take_padded(ref, k):
+        for j in range(ns):
+            returned[j * pad : j * pad + cap] = ref[k, j]
+        return returned[...].astype(jnp.float32)
+
+    summed = sum_over_tp(
+        part_block, put_groups, take_padded, part_out, part_in, part_yout, part_yin, part_sem
+    )
+    put_groups(back_out, 0, summed)
+    backs = []
+    for hop in range(1, ns):
+        to = lax.rem(sp + hop, ns)
+        backs.append(send(back_out.at[0, to], back_in.at[sp], back_sem, (hop - 1,), {"sp": to}))
+    back_in[sp] = back_out[0, sp]
+    for copy in backs:
+        copy.wait_recv()
+    for j in range(ns):
+        returned[j * pad : j * pad + cap] = back_in[j]
+    mixture = dot(pick_t_ref[...], returned[...])
+    result = normed(ALPHA * middle.astype(jnp.float32) + mixture, last_gain_ref[...], 1)
+    out_ref[...] = result.astype(out_ref.dtype)
+    for copy in waits:
+        copy.wait_send()
+
+
+def layer(heads_out, wo, rows, gain, last_gain, pick, pick_t, info, weights, cap, pad, cid):
+    ns, nt = lax.axis_size("sp"), lax.axis_size("tp")
+    chips = nt // 2
+    tokens, width = rows.shape
+    wv, wr, wd, cv, cr, cd = weights
+    half, dma = jnp.bfloat16, pltpu.SemaphoreType.DMA
+    across = max(chips - 1, 1)
+
+    def vm(*shape, dtype=half):
+        return pltpu.VMEM(shape, dtype)
+
+    scratch = [
+        vm(*wv.shape[1:]), vm(*wr.shape[1:]), vm(*wd.shape[1:]),
+        vm(*cv.shape), vm(*cr.shape), vm(*cd.shape), dma((6,)),
+        vm(chips, tokens, width), vm(chips, tokens, width),
+        vm(across, tokens, width), vm(across, tokens, width), dma((2, 2 * chips)),
+        vm(2, 8, tokens, dtype=jnp.float32), vm(2, nt - 1, 8, tokens, dtype=jnp.float32),
+        dma((2, 2, nt - 1)),
+        vm(ns, cap, width), vm(nt, ns, cap, width), vm(ns, 8, 128, dtype=jnp.float32),
+        dma((2, ns - 1)), dma((2, ns - 1)), dma((2, ns, across)), dma((2, ns, chips)),
+        vm(ns * pad, width * nt), vm(ns * pad, wv.shape[2]), vm(ns * pad, cv.shape[1]),
+        vm(ns * pad, 128, dtype=jnp.float32),
+        vm(chips, ns, cap, width), vm(chips, ns, cap, width),
+        vm(across, ns, cap, width), vm(across, ns, cap, width), dma((2, 2 * chips)),
+        vm(1, ns, cap, width), vm(ns, cap, width), dma((2, ns - 1)), vm(ns * pad, width),
+    ]
+    return pl.pallas_call(
+        functools.partial(layer_kernel, ns, nt, cap, pad),
+        out_shape=jax.ShapeDtypeStruct((tokens, width), half),
+        in_specs=vmem_specs(8) + [pl.BlockSpec(memory_space=pl.ANY)] * 6,
+        out_specs=pl.BlockSpec(memory_space=pltpu.VMEM),
+        scratch_shapes=scratch,
+        compiler_params=pltpu.CompilerParams(
+            collective_id=cid, has_side_effects=True, vmem_limit_bytes=60 * 2**20
+        ),
+        name="layer",
+    )(heads_out, wo, rows, gain, last_gain, pick, pick_t, info, *weights)
 
 
 def block_pass(query_unit, key_unit, write_gate, decay_logarithm, segment, values_in, initial):
@@ -357,12 +613,6 @@
     heads_out = (token_major * jax.nn.silu(exit_valve_raw_signal.astype(jnp.float32))).astype(
         jnp.bfloat16
     )
-    partial_proj = jnp.dot(heads_out, final_projection_matrix, preferred_element_type=jnp.float32)
-    (shares,) = exchange((partial_proj.astype(jnp.bfloat16),), ("cols",), "tp", 2)
-    projected = jnp.sum(shares.astype(jnp.float32), 0)
-    middle = feature_norm(
-        ALPHA * incoming_rows_matrix.astype(jnp.float32) + projected, initial_rescale_factor, 3
-    ).astype(jnp.bfloat16)
     top = specialist_picks.shape[1]
     local_experts = specialist_valve_matrix.shape[0]
     experts_all = local_experts * lax.axis_size("sp")
@@ -373,59 +623,41 @@
         jnp.int32
     )
     rank_in = jnp.sum(jnp.cumsum(one_hot, 0) * one_hot, 1) - 1
-    slot_of = flat_routes * capacity + rank_in
-    slots = experts_all * capacity
-    slot_table = slot_of.reshape(tokens_here, top)
-    matches = [
-        jnp.arange(slots, dtype=jnp.int32)[:, None] == slot_table[None, :, j] for j in range(top)
-    ]
+    pad = -(-capacity // 16) * 16
+    slot_table = (flat_routes * pad + rank_in).reshape(tokens_here, top)
+    order = jnp.arange(experts_all * pad, dtype=jnp.int32)
+    matches = [order[:, None] == slot_table[None, :, j] for j in range(top)]
     pick = functools.reduce(jnp.logical_or, matches).astype(jnp.bfloat16)
+    turned = [order[None, :] == slot_table[:, j, None] for j in range(top)]
+    pick_t = functools.reduce(jnp.logical_or, turned).astype(jnp.bfloat16)
     slot_weight = sum(
-        jnp.sum(
-            jnp.where(matches[j], picked_specialist_share[None, :, j].astype(jnp.float32), 0.0), 1
-        )
+        jnp.sum(jnp.where(turned[j], picked_specialist_share[:, j, None].astype(jnp.float32), 0.0), 0)
         for j in range(top)
     )
-    slot_shared = jnp.any(matches[0], 1).astype(jnp.float32)
-    slot_info = jnp.stack([slot_weight, slot_shared]).astype(jnp.bfloat16)
-    slot_info = jnp.moveaxis(slot_info.reshape(2, experts_all, capacity), 0, 1)
-    sp_size = lax.axis_size("sp")
-    slot_count = capacity * local_experts
-    sent = jnp.dot(pick, middle, preferred_element_type=jnp.float32).astype(jnp.bfloat16)
-    arrived, info = exchange(
-        (sent.reshape(sp_size, slot_count, -1), slot_info.reshape(sp_size, local_experts * 2, capacity)),
-        ("rows", "rows"),
-        "sp",
-        5,
-    )
-    sources = sp_size
-    (inputs_e,) = exchange((arrived.reshape(sources * slot_count, -1),), ("join",), "tp", 6)
-    info = info.astype(jnp.float32)
-    weight_e = info[:, 0].reshape(-1, 1)
-    shared_e = info[:, 1].reshape(-1, 1)
-    gate_e = jnp.dot(inputs_e, specialist_valve_matrix[0], preferred_element_type=jnp.float32)
-    up_e = jnp.dot(inputs_e, specialist_raising_matrix[0], preferred_element_type=jnp.float32)
-    hidden_e = (jax.nn.silu(gate_e) * up_e * weight_e).astype(jnp.bfloat16)
-    shared_g = jnp.dot(inputs_e, common_valve_matrix, preferred_element_type=jnp.float32)
-    shared_u = jnp.dot(inputs_e, common_raising_matrix, preferred_element_type=jnp.float32)
-    shared_hidden = (jax.nn.silu(shared_g) * shared_u * shared_e).astype(jnp.bfloat16)
-    partial_out = jnp.dot(
-        hidden_e, specialist_lowering_matrix[0], preferred_element_type=jnp.float32
-    )
-    partial_out = partial_out + jnp.dot(
-        shared_hidden, common_lowering_matrix, preferred_element_type=jnp.float32
-    )
-    (pieces,) = exchange((partial_out.astype(jnp.bfloat16),), ("cols",), "tp", 7)
-    summed = jnp.sum(pieces.astype(jnp.float32), 0).astype(jnp.bfloat16)
-    (returned,) = exchange((summed.reshape(sources, slot_count, -1),), ("rows",), "sp", 8)
-    mixture = lax.dot_general(
+    slot_shared = jnp.any(turned[0], 0).astype(jnp.float32)
+    info = jnp.stack([slot_weight, slot_shared]).reshape(2, experts_all, pad)
+    info = jnp.pad(jnp.moveaxis(info, 0, 1), ((0, 0), (0, 6), (0, 128 - pad)))
+    return layer(
+        heads_out,
+        final_projection_matrix,
+        incoming_rows_matrix,
+        initial_rescale_factor[None, :],
+        latter_rescale_factor[None, :],
         pick,
-        returned.reshape(slots, -1),
-        (((0,), (0,)), ((), ())),
-        preferred_element_type=jnp.float32,
-    )
-    second_sum = ALPHA * middle.astype(jnp.float32) + mixture
-    return feature_norm(second_sum, latter_rescale_factor, 4).astype(jnp.bfloat16)
+        pick_t,
+        info,
+        (
+            specialist_valve_matrix,
+            specialist_raising_matrix,
+            specialist_lowering_matrix,
+            common_valve_matrix,
+            common_raising_matrix,
+            common_lowering_matrix,
+        ),
+        capacity,
+        pad,
+        2,
+    )
 
 
 def solution(mesh):

time: 177 us -> 117 us (0.66)
  Pallas kernels: 112 us -> 89.6 us
  matrix products: 30.7 us -> 8.66 us
  local copies, waits for them, and re-layouts: 16.6 us -> 8.27 us
  other arithmetic: 15 us -> 9.17 us
    pallas_call x8 -> x1, Pallas kernels: 98.9 us -> 9.55 us  [exchange(): pl.pallas_call(functools.partial(exchange_kernel, axis, n, modes), out_sh...]
    pallas_call x0 -> x1, Pallas kernels: none -> 66.8 us  [layer(): pl.pallas_call(functools.partial(layer_kernel, ns, nt, cap, pad), out_sha...]
    dot_general x7 -> x0, matrix products: 20.8 us -> none  [the longest x1 7.94 us: shards(): jnp.dot(hidden_e, specialist_lowering_matrix[0], preferred_element_type=j...]
    reshape x4 -> x0, local copies, waits for them, and re-layouts: 4.33 us -> none  [the longest x1 1.75 us: shards(): arrived.reshape(sources * slot_count, -1)]
    reduce_sum x6 -> x1, other arithmetic: 4.4 us -> 0.15 us  [shards(): jnp.sum(jnp.where(turned[j], picked_specialist_share[:, j, None].astype(j...]
    while x12 -> x0, local copies, waits for them, and re-layouts: 3.01 us -> none
where the time goes in v2:
time: 117 us
  Pallas kernels  89.6 us (77%)
  other arithmetic  9.17 us (8%)
  matrix products  8.66 us (7%)
  local copies, waits for them, and re-layouts  8.27 us (7%)
    pallas_call x1, Pallas kernels, layer(): pl.pallas_call(functools.partial(layer_kernel, ns, nt, cap, pad), out_sha...  66.8 us
    pallas_call x1, Pallas kernels, entering(): pl.pallas_call(functools.partial(scan_kernel, n, hops), out_shape=jax.Sha...  13.3 us
    pallas_call x1, Pallas kernels, exchange(): pl.pallas_call(functools.partial(exchange_kernel, axis, n, modes), out_sh...  9.55 us
    dot_general x11, matrix products, matmul_high(): return jnp.einsum(form, left, right, precision=HIGH)  4.62 us
    dot_general x12, matrix products, matmul_one(): jnp.einsum(form, left.astype(jnp.bfloat16), right.astype(jnp.bfloat16), p...  4.04 us
    unnamed x16, local copies, waits for them, and re-layouts  2.86 us

profile of v2, /device:TPU:0, one launch (start us, length us, event | category | flops | bytes accessed | tf_op | source)
XLA Modules:
  0.0 117.0 jit_solution(17514677199043823098)
XLA Ops:
  0.0 0.7 convert_element_type.139
  0.9 1.0 copy.80
  2.2 0.7 exp.37
  2.8 0.8 fusion.66
  3.7 0.9 reduce_window_sum.26
  4.6 0.7 add_divide_fusion
  5.4 0.7 fusion.19
  6.2 0.4 fusion.70
  6.6 0.4 fusion.35
  7.0 0.4 fusion.71
  7.4 0.4 fusion.33
  8.2 0.4 fusion.31
  9.0 0.4 fusion.29
  9.4 0.4 convolution_add_fusion.3
  9.8 0.4 convolution_convert_fusion
  10.2 0.7 fusion.69
  11.0 1.4 %compare_convert_fusion.2 = (f32[2]{0:T(128)S(1)}, f32[2]{0:T(128)S(1)}) fusion(f32[2]{0:T(128)S(1)} %slice_reduce_fusion.1, f32[1]{0:T(128)} %bitcast.9, f32[1]{0:T(128)} %bitcast.8), kind=kLoop, calls=%fused_computation.122 | loop fusion | flops 6 | bytes 32 | tf_op jit(solution)/shard_map/convert_element_type | solution.py:517
  12.8 0.4 convolution_bitcast_fusion.2
  15.0 1.9 %while.12 = (s32[]{:T(128)}, f32[4,128,256]{2,1,0:T(8,128)S(1)}, f32[2,4,64,256]{3,2,1,0:T(8,128)S(1)}, f32[2,4]{1,0:T(2,128)S(1)}, bf16[2,4,64,128]{3,2,0,1:T(8...) while((s32[]{:T(128)}, f32[4,128,256]{2,1,0:T(8,128)S(1)}, ...), condition=%wide.region_4.5_spmd, body=%wide.region_3.4_spmd.sunk | while | flops 59441152 | bytes 3803793 | solution.py:542
  16.9 9.5 %exchange_sp_0.1 = s32[8,1,128]{2,1,0:T(1,128)} custom-call(s32[1,128]{1,0:T(1,128)} %bitcast.178), custom_call_target="tpu_custom_call" | custom-call | tf_op jit(solution)/shard_map/exchange_sp_0/pallas_call | solution.py:89
  26.4 0.8 slice.61
  27.2 0.5 constant_dynamic-slice_fusion.1
  28.4 0.7 pad_maximum_fusion.own_ref
  29.1 13.3 %state_scan.1 = f32[4,128,128]{2,1,0:T(8,128)} custom-call(bf16[2,4,128,128]{3,2,1,0:T(8,128)(2,1)} %pad_maximum_fusion.own_ref), custom_call_target="tpu_custom_call" | custom-call | tf_op jit(solution)/shard_map/state_scan/pallas_call | solution.py:198
  42.5 1.3 %multiply_reduce_fusion = (f32[4,128]{1,0:T(4,128)S(1)}, f32[4,128,128]{2,1,0:T(8,128)S(1)}) fusion(f32[4,128,128]{2,1,0:T(8,128)} %state_scan.1, f32[]{:T(128)S(6)} %convert_element_type.149, f32[4,128,256]{2,1,0:T(8,128)S(1)} %bitcast.164), kind=kOutput, calls=%fused_computation.48 | convolution fusion | flops 17169920 | bytes 1050628 | tf_op jit(solution)/shard_map/hcd,hde->hce/dot_general | solution.py:219
  43.8 0.8 fusion.38.heads_ref
  44.9 0.6 reduce-window.6
  46.5 0.8 fusion.41
  47.3 0.6 pad.7.info_ref
  47.9 0.7 fusion.44.pick_ref
  48.6 66.8 %layer.1 = bf16[128,512]{1,0:T(8,128)(2,1)} custom-call(bf16[128,512]{1,0:T(8,128)(2,1)} %fusion.38.heads_ref, bf16[512,2048]{1,0:T(8,128)(2,1)} %wo_ref.1, bf16[128,512]{1,0:T(8,128)(2,1)} %rows_ref.1, f32[1,512]{1,0:T(1,128)} %bitcast.176, f32[1,512]{1,0:T(1,128)} %bitcast.177, bf16[384,128]{1,0:T(8,128)(2,1)} %fusion.44.pick_ref, ...), custom_call_target="tpu_custom_call" | custom-call | tf_op jit(solution)/shard_map/layer/pallas_call | solution.py:480
  115.4 1.6 %copy.120 = bf16[128,512]{1,0:T(8,128)(2,1)} copy(bf16[128,512]{1,0:T(8,128)(2,1)} %layer.1) | data formatting | bytes 262144
  (81 shorter events, 6.8 us)
Async XLA Ops:
  6.2 7.1 %copy-start = (bf16[128,512]{1,0:T(8,128)(2,1)S(1)}, bf16[128,512]{1,0:T(8,128)(2,1)}, u32[]{:S(2)}) copy-start(bf16[128,512]{1,0:T(8,128)(2,1)} %param.25) | copy-start | bytes 393220
  7.0 6.7 %copy-start.1 = (bf16[128,512]{1,0:T(8,128)(2,1)S(1)}, bf16[128,512]{1,0:T(8,128)(2,1)}, u32[]{:S(2)}) copy-start(bf16[128,512]{1,0:T(8,128)(2,1)} %param.23) | copy-start | bytes 393220
  14.9 12.8 %copy-start.5 = (s32[128]{0:T(128)S(1)}, s32[128]{0:T(128)}, u32[]{:S(2)}) copy-start(s32[128]{0:T(128)} %param.30) | copy-start | bytes 1540
  14.9 28.8 %copy-start.2 = (bf16[128,512]{1,0:T(8,128)(2,1)S(1)}, bf16[128,512]{1,0:T(8,128)(2,1)}, u32[]{:S(2)}) copy-start(bf16[128,512]{1,0:T(8,128)(2,1)} %param.31) | copy-start | bytes 393220
  15.0 29.6 %copy-start.3 = (s32[128,2]{0,1:T(2,128)S(1)}, s32[128,2]{0,1:T(2,128)}, u32[]{:S(2)}) copy-start(s32[128,2]{0,1:T(2,128)} %param.35) | copy-start | bytes 3076
  16.9 29.3 %copy-start.4 = (bf16[128,2]{0,1:T(2,128)(2,1)S(1)}, bf16[128,2]{0,1:T(2,128)(2,1)}, u32[]{:S(2)}) copy-start(bf16[128,2]{0,1:T(2,128)(2,1)} %param.36) | copy-start | bytes 1540

commit v3 on v2

--- a/solution.py
+++ b/solution.py
@@ -20,85 +20,6 @@
 
 def vmem_specs(count):
     return [pl.BlockSpec(memory_space=pltpu.VMEM)] * count
-
-
-def exchange_kernel(axis, n, modes, *refs):
-    count = len(modes)
-    ins, outs = refs[:count], refs[count : 2 * count]
-    send_sem, recv_sem, own_sem = refs[2 * count :]
-    me = lax.axis_index(axis)
-    barrier = pltpu.get_barrier_semaphore()
-    for hop in range(1, n):
-        pl.semaphore_signal(
-            barrier, inc=1, device_id={axis: lax.rem(me + hop, n)}, device_id_type=MESH
-        )
-
-    def span(ref, place, size):
-        return ref.at[:, pl.ds(pl.multiple_of(place * size, size), size)]
-
-    def ends(index, target):
-        source, landing = ins[index], outs[index]
-        if modes[index] == "rows":
-            return source.at[target], landing.at[me]
-        if modes[index] == "cols":
-            return span(source, target, landing.shape[-1]), landing.at[me]
-        if modes[index] == "join":
-            return source, span(landing, me, source.shape[-1])
-        return source, landing.at[me]
-
-    own = []
-    for index in range(count):
-        source, landing = ends(index, me)
-        own.append(pltpu.make_async_copy(source, landing, own_sem.at[index]))
-        own[-1].start()
-    pl.semaphore_wait(barrier, n - 1)
-    sent = []
-    for hop in range(1, n):
-        target = lax.rem(me + hop, n)
-        for index in range(count):
-            source, landing = ends(index, target)
-            sent.append(
-                pltpu.make_async_remote_copy(
-                    src_ref=source,
-                    dst_ref=landing,
-                    send_sem=send_sem.at[index, hop - 1],
-                    recv_sem=recv_sem.at[index, hop - 1],
-                    device_id={axis: target},
-                    device_id_type=MESH,
-                )
-            )
-            sent[-1].start()
-    for copy in own + sent:
-        copy.wait()
-
-
-def exchange(arrays, modes, axis, cid):
-    n = lax.axis_size(axis)
-    count = len(arrays)
-    shapes = []
-    for array, mode in zip(arrays, modes):
-        if mode == "rows":
-            shape = array.shape
-        elif mode == "cols":
-            shape = (n, array.shape[0], array.shape[1] // n)
-        elif mode == "join":
-            shape = (array.shape[0], array.shape[1] * n)
-        else:
-            shape = (n,) + array.shape
-        shapes.append(jax.ShapeDtypeStruct(shape, array.dtype))
-    return pl.pallas_call(
-        functools.partial(exchange_kernel, axis, n, modes),
-        out_shape=shapes,
-        in_specs=vmem_specs(count),
-        out_specs=vmem_specs(count),
-        scratch_shapes=[
-            pltpu.SemaphoreType.DMA((count, n - 1)),
-            pltpu.SemaphoreType.DMA((count, n - 1)),
-            pltpu.SemaphoreType.DMA((count,)),
-        ],
-        compiler_params=pltpu.CompilerParams(collective_id=cid, has_side_effects=True),
-        name=f"exchange_{axis}_{cid}",
-    )(*arrays)
 
 
 def scan_plan(n, reach):
@@ -113,10 +34,10 @@
     return hops
 
 
-def scan_kernel(n, hops, own_ref, out_ref, *scratch):
+def scan_kernel(n, hops, own_ref, label_ref, out_ref, *scratch):
     rounds = len(hops)
     landed, built = scratch[:rounds], scratch[rounds : 2 * rounds]
-    send_sem, recv_sem = scratch[2 * rounds :]
+    send_sem, recv_sem, label_in, label_sem = scratch[2 * rounds :]
     heads = own_ref.shape[1]
     me = lax.axis_index("sp")
     barrier = pltpu.get_barrier_semaphore()
@@ -131,7 +52,7 @@
 
     def copy_of(index):
         last = index == rounds - 1 and index > 1
-        source = own_ref if index == 0 else built[index]
+        source = built[index]
         landing = landed[index]
         if last:
             source, landing = source.at[1], landing.at[1]
@@ -144,6 +65,21 @@
             device_id_type=MESH,
         )
 
+    note = pltpu.make_async_remote_copy(
+        src_ref=label_ref,
+        dst_ref=label_in,
+        send_sem=label_sem.at[0],
+        recv_sem=label_sem.at[1],
+        device_id={"sp": lax.rem(me + 1, n)},
+        device_id_type=MESH,
+    )
+    note.start()
+    note.wait_recv()
+    before, first = label_in[0:1, label_in.shape[1] - 1 :], label_ref[0:1, 0:1]
+    joined = ((before == first) & (me > 0)).astype(jnp.float32)
+    for h in range(heads):
+        built[0][0, h] = (own_ref[0, h] * joined).astype(built[0].dtype)
+        built[0][1, h] = own_ref[1, h].astype(built[0].dtype)
     window = None
     for index, hop in enumerate(hops):
         copy = copy_of(index)
@@ -164,9 +100,9 @@
         got = landed[index]
         if index == 0:
             if last:
-                out_ref[...] = got[1].astype(jnp.float32)
+                out_ref[...] = got[1].astype(jnp.float32) * joined
             else:
-                later, target = own_ref, built[1]
+                later, target = built[0], built[1]
                 for h in range(heads):
                     target[0, h] = dot(later[0, h], got[0, h]).astype(target.dtype)
                     target[1, h] = (
@@ -177,7 +113,7 @@
             for h in range(heads):
                 shift = dot(window[0, h], got[1, h]) + window[1, h].astype(jnp.float32)
                 if last:
-                    out_ref[h] = shift
+                    out_ref[h] = shift * joined
                 else:
                     target = built[index + 1]
                     target[0, h] = dot(window[0, h], got[0, h]).astype(target.dtype)
@@ -190,21 +126,24 @@
         def _():
             copy_of(index).wait_send()
 
-
-def entering(summary, reach, cid):
+    note.wait_send()
+
+
+def entering(summary, labels, reach, cid):
     n = lax.axis_size("sp")
     hops = scan_plan(n, reach)
-    block = pltpu.VMEM(summary.shape, summary.dtype)
+    block = pltpu.VMEM(summary.shape, jnp.bfloat16)
     return pl.pallas_call(
         functools.partial(scan_kernel, n, hops),
         out_shape=jax.ShapeDtypeStruct(summary.shape[1:], jnp.float32),
-        in_specs=vmem_specs(1),
+        in_specs=vmem_specs(2),
         out_specs=pl.BlockSpec(memory_space=pltpu.VMEM),
         scratch_shapes=[block] * (2 * len(hops))
-        + [pltpu.SemaphoreType.DMA((len(hops),)), pltpu.SemaphoreType.DMA((len(hops),))],
+        + [pltpu.SemaphoreType.DMA((len(hops),)), pltpu.SemaphoreType.DMA((len(hops),))]
+        + [pltpu.VMEM(labels.shape, labels.dtype), pltpu.SemaphoreType.DMA((2,))],
         compiler_params=pltpu.CompilerParams(collective_id=cid, has_side_effects=True),
         name="state_scan",
-    )(summary)
+    )(summary, labels)
 
 
 def unit_rows(array):
@@ -596,13 +535,9 @@
     summary, local_out = block_pass(
         query_unit, key_unit, write_gate, decay_logarithm, segment, extended, start_state
     )
-    (edges,) = exchange((sequence_label[None, :],), ("all",), "sp", 0)
-    place = lax.axis_index("sp")
-    before = lax.dynamic_index_in_dim(edges[:, 0, -1], jnp.maximum(place - 1, 0), 0, False)
-    joined = ((before == sequence_label[0]) & (place > 0)).astype(jnp.float32)
     reach = -(-(DOC_SPAN - 1) // tokens_here)
-    own = jnp.stack([summary[..., DV:] * joined, summary[..., :DV]]).astype(jnp.bfloat16)
-    incoming = entering(own, reach, 1) * joined
+    own = jnp.stack([summary[..., DV:], summary[..., :DV]])
+    incoming = entering(own, sequence_label[None, :], reach, 1)
     memory_layer_result = local_out[..., :DV] + matmul_one(
         "hcd,hde->hce", local_out[..., DV:], incoming
     )

time: 117 us -> 112 us (0.957)
  Pallas kernels: 89.6 us -> 85.8 us
  local copies, waits for them, and re-layouts: 8.27 us -> 7.01 us
    pallas_call x1 -> x0, Pallas kernels: 9.55 us -> none  [exchange(): pl.pallas_call(functools.partial(exchange_kernel, axis, n, modes), out_sh...]
    pallas_call x1, Pallas kernels: 13.3 us -> 17.8 us  [entering(): pl.pallas_call(functools.partial(scan_kernel, n, hops), out_shape=jax.Sha...]
    pallas_call x1, Pallas kernels: 66.8 us -> 68 us  [layer(): pl.pallas_call(functools.partial(layer_kernel, ns, nt, cap, pad), out_sha...]
    unnamed x16 -> x14, local copies, waits for them, and re-layouts: 2.86 us -> 2.85 us
where the time goes in v3:
time: 112 us; the launch traced here: 111 us
  Pallas kernels  85.8 us (77%)
  other arithmetic  9.26 us (8%)
  matrix products  8.66 us (8%)
  local copies, waits for them, and re-layouts  7.01 us (6%)
    pallas_call x1, Pallas kernels, layer(): pl.pallas_call(functools.partial(layer_kernel, ns, nt, cap, pad), out_sha...  68 us
    pallas_call x1, Pallas kernels, entering(): pl.pallas_call(functools.partial(scan_kernel, n, hops), out_shape=jax.Sha...  17.8 us
    dot_general x11, matrix products, matmul_high(): return jnp.einsum(form, left, right, precision=HIGH)  4.62 us
    dot_general x12, matrix products, matmul_one(): jnp.einsum(form, left.astype(jnp.bfloat16), right.astype(jnp.bfloat16), p...  4.03 us
    unnamed x14, local copies, waits for them, and re-layouts  2.85 us

profile of v3, /device:TPU:0, one launch (start us, length us, event | category | flops | bytes accessed | tf_op | source)
XLA Modules:
  0.0 111.2 jit_solution(9839226872799702178)
XLA Ops:
  0.0 0.7 convert_element_type.135
  0.9 1.0 copy.80
  2.2 0.7 exp.37
  2.8 0.8 fusion.64
  3.7 0.9 reduce_window_sum.26
  4.6 0.7 add_divide_fusion
  5.4 0.7 fusion.19
  6.2 0.4 fusion.68
  6.6 0.4 fusion.35
  7.0 0.4 fusion.69
  7.4 0.4 fusion.33
  7.8 0.4 fusion.70
  8.2 0.4 fusion.31
  8.6 0.4 fusion.71
  9.0 0.4 fusion.29
  9.4 0.4 convolution_add_fusion.3
  9.8 0.4 convolution_convert_fusion
  10.2 0.7 fusion.67
  11.0 1.4 %compare_convert_fusion.2 = (f32[2]{0:T(128)S(1)}, f32[2]{0:T(128)S(1)}) fusion(f32[2]{0:T(128)S(1)} %slice_reduce_fusion.1, f32[1]{0:T(128)} %bitcast.9, f32[1]{0:T(128)} %bitcast.8), kind=kLoop, calls=%fused_computation.119 | loop fusion | flops 6 | bytes 32 | tf_op jit(solution)/shard_map/convert_element_type | solution.py:456
  12.8 0.4 convolution_bitcast_fusion.2
  14.9 1.9 %while.12 = (s32[]{:T(128)}, f32[4,128,256]{2,1,0:T(8,128)S(1)}, f32[2,4,64,256]{3,2,1,0:T(8,128)S(1)}, f32[2,4]{1,0:T(2,128)S(1)}, bf16[2,4,64,128]{3,2,0,1:T(8...) while((s32[]{:T(128)}, f32[4,128,256]{2,1,0:T(8,128)S(1)}, ...), condition=%wide.region_4.5_spmd, body=%wide.region_3.4_spmd.sunk | while | flops 59441152 | bytes 3803793 | solution.py:481
  15.5 0.4 convolution_add_fusion.5
  16.9 0.8 pad_maximum_fusion.own_ref
  17.7 17.8 %state_scan.1 = f32[4,128,128]{2,1,0:T(8,128)} custom-call(f32[2,4,128,128]{3,2,1,0:T(8,128)} %pad_maximum_fusion.own_ref, s32[1,128]{1,0:T(1,128)} %bitcast.175), custom_call_target="tpu_custom_call" | custom-call | tf_op jit(solution)/shard_map/state_scan/pallas_call | solution.py:136
  35.6 1.2 %multiply_reduce_fusion = (f32[4,128]{1,0:T(4,128)S(1)}, f32[4,128,128]{2,1,0:T(8,128)S(1)}) fusion(f32[4,128,128]{2,1,0:T(8,128)} %state_scan.1, f32[4,128,256]{2,1,0:T(8,128)S(1)} %bitcast.159), kind=kOutput, calls=%fused_computation.47 | convolution fusion | flops 17104384 | bytes 1050624 | tf_op jit(solution)/shard_map/hcd,hde->hce/dot_general | solution.py:158
  36.9 0.8 fusion.38.heads_ref
  37.9 0.6 reduce-window.6
  39.5 0.8 fusion.41
  40.4 0.6 pad.7.info_ref
  41.0 0.7 fusion.44.pick_ref
  41.7 68.0 %layer.1 = bf16[128,512]{1,0:T(8,128)(2,1)} custom-call(bf16[128,512]{1,0:T(8,128)(2,1)} %fusion.38.heads_ref, bf16[512,2048]{1,0:T(8,128)(2,1)} %wo_ref.1, bf16[128,512]{1,0:T(8,128)(2,1)} %rows_ref.1, f32[1,512]{1,0:T(1,128)} %bitcast.173, f32[1,512]{1,0:T(1,128)} %bitcast.174, bf16[384,128]{1,0:T(8,128)(2,1)} %fusion.44.pick_ref, ...), custom_call_target="tpu_custom_call" | custom-call | tf_op jit(solution)/shard_map/layer/pallas_call | solution.py:419
  109.7 1.6 %copy.120 = bf16[128,512]{1,0:T(8,128)(2,1)} copy(bf16[128,512]{1,0:T(8,128)(2,1)} %layer.1) | data formatting | bytes 262144
  (75 shorter events, 5.6 us)
Async XLA Ops:
  6.2 7.1 %copy-start = (bf16[128,512]{1,0:T(8,128)(2,1)S(1)}, bf16[128,512]{1,0:T(8,128)(2,1)}, u32[]{:S(2)}) copy-start(bf16[128,512]{1,0:T(8,128)(2,1)} %param.25) | copy-start | bytes 393220
  7.0 6.6 %copy-start.1 = (bf16[128,512]{1,0:T(8,128)(2,1)S(1)}, bf16[128,512]{1,0:T(8,128)(2,1)}, u32[]{:S(2)}) copy-start(bf16[128,512]{1,0:T(8,128)(2,1)} %param.23) | copy-start | bytes 393220
  16.8 20.0 %copy-start.2 = (bf16[128,512]{1,0:T(8,128)(2,1)S(1)}, bf16[128,512]{1,0:T(8,128)(2,1)}, u32[]{:S(2)}) copy-start(bf16[128,512]{1,0:T(8,128)(2,1)} %param.31) | copy-start | bytes 393220
  16.8 20.8 %copy-start.3 = (s32[128,2]{0,1:T(2,128)S(1)}, s32[128,2]{0,1:T(2,128)}, u32[]{:S(2)}) copy-start(s32[128,2]{0,1:T(2,128)} %param.35) | copy-start | bytes 3076
  16.8 22.4 %copy-start.4 = (bf16[128,2]{0,1:T(2,128)(2,1)S(1)}, bf16[128,2]{0,1:T(2,128)(2,1)}, u32[]{:S(2)}) copy-start(bf16[128,2]{0,1:T(2,128)(2,1)} %param.36) | copy-start | bytes 1540
